TPU v7x, 512 devices: a whole 4x8x8 slice. The times are simulated.
512 devices in a mesh: sp: 128 (over z, y, core), tp: 4 (over x).
Axes of the slice: x: 4, y: 8, z: 8, core: 2. Of those that a mesh axis runs over, the one named last changes fastest.
Arguments:
- tokens: bfloat16 [65536, 2048], P('sp'), may hold values from -6 to 6
- norm_gain: float32 [2048], replicated, may hold values from 0.1 to 1.9
- w_value: bfloat16 [2048, 512], P('sp', 'tp'), may hold values from -0.125 to 0.125
- w_gate: bfloat16 [2048, 512], P('sp', 'tp'), may hold values from -0.125 to 0.125
- w_drive: bfloat16 [2048, 512], P('sp', 'tp'), may hold values from -0.125 to 0.125
- conv_taps: float32 [31, 512], P(None, 'tp'), may hold values from -12 to 12
- conv_gain: float32 [512], P('tp'), may hold values from 0.1 to 1.9
- log_step: float32 [32], P('tp'), may hold values from -20 to -3
- step_shift: float32 [65536, 32], P('sp', 'tp'), may hold values from -1.5 to 12
- state_real: float32 [32, 64], P('tp'), may hold values from -1.2 to -0.5
- state_imag: float32 [32, 64], P('tp'), may hold values from 0 to 201.06177
- in_map: float32 [2, 32, 64, 16], P(None, 'tp'), may hold values from -6 to 6
- out_map: float32 [2, 32, 16, 64], P(None, 'tp'), may hold values from -1.5 to 1.5
- skip_gain: float32 [32, 16], P('tp'), may hold values from -3 to 3
- start_state: float32 [2, 32, 64], P(None, 'tp'), may hold values from -6 to 6
- conv_proj: bfloat16 [512, 2048], P('tp', 'sp'), may hold values from -0.1875 to 0.1875
- state_proj: bfloat16 [512, 2048], P('tp', 'sp'), may hold values from -0.1875 to 0.1875
Outputs:
- mixed: bfloat16 [65536, 2048], P('sp', 'tp')
All inputs are finite; a program needn't handle non-finite values.
Results may differ from a plain program's by a relative error of at most 0.013.
Values may be sent and summed in bfloat16 or wider, within the bound.
A program may use at most 64 MiB of HBM per device.

v0:
```python
import math

import jax
import jax.numpy as jnp
from jax import lax
from jax.sharding import Mesh
from jax.sharding import PartitionSpec as P

SP = ("sp_0", "sp_1", "sp_2")


def sent_together(arrays, axis, dim, along):
    widths = [a.shape[along] for a in arrays]
    both = jnp.concatenate(arrays, axis=along)
    out = lax.all_gather(both, axis, axis=dim, tiled=True)
    return tuple(jnp.split(out, [sum(widths[:k]) for k in range(1, len(widths))], axis=along))


def from_behind(x, axis, by):
    devices = lax.axis_size(axis)
    pairs = [(i, i + by) for i in range(devices) if 0 <= i + by < devices]
    return lax.ppermute(x, axis, pairs)


def sent_to_all(x, axis):
    copies = jnp.broadcast_to(x, (lax.axis_size(axis), *x.shape))
    return lax.all_to_all(copies, axis, split_axis=0, concat_axis=0, tiled=True)


def of_everyone(x, axis):
    return sent_to_all(x, axis).sum(axis=0)


def packed_total(arrays, axis):
    vector, at, finished = (jnp.concatenate([a.reshape(-1) for a in arrays]), 0, [])
    total = of_everyone(vector, axis)
    for a in arrays:
        finished.append(total[at : at + a.size].reshape(a.shape))
        at += a.size
    return tuple(finished)


def nothing_yet(x, identity):
    return jax.tree.map(
        lambda part, zero: jnp.zeros_like(part) + jnp.asarray(zero, part.dtype), x, identity
    )


def gathered_once(x, axis):
    leaves = jax.tree.leaves(x)
    sequence = sorted(range(len(leaves)), key=lambda k: -leaves[k].size)
    width = (1, *leaves[sequence[0]].shape)[-1]
    lines = [
        jnp.pad(leaves[k].reshape(-1), (0, -leaves[k].size % width)).reshape(-1, width)
        for k in sequence
    ]
    both, at, found = (lax.all_gather(jnp.concatenate(lines), axis), 0, {})
    for k, line in zip(sequence, lines):
        piece = both[:, at : at + len(line)].reshape(len(both), -1)
        found[k] = piece[:, : leaves[k].size].reshape(-1, *leaves[k].shape)
        at += len(line)
    numbers = iter(range(len(leaves)))
    return jax.tree.map(lambda _: found[next(numbers)], x)


def carried_in(x, axes, combine, identity):
    before = start = nothing_yet(x, identity)
    total = x
    for axis in reversed(axes):
        devices, mine = (lax.axis_size(axis), lax.axis_index(axis))
        pieces = gathered_once(total, axis)
        inside, total = (start, start)
        for k in range(devices):
            passed = k < mine
            total = combine(total, jax.tree.map(lambda part: part[k], pieces))
            inside = jax.tree.map(lambda new, old: jnp.where(passed, new, old), total, inside)
        before = combine(inside, before)
    return before


def split_up(x, dim, devices):
    lengths = x.shape
    pieces = x.reshape(*lengths[:dim], devices, lengths[dim] // devices, *lengths[dim + 1 :])
    return jnp.moveaxis(pieces, dim, 0)


def sent_and_summed(x, axis, dim):
    pieces = split_up(x, dim, lax.axis_size(axis))
    arrived = lax.all_to_all(pieces, axis, split_axis=0, concat_axis=0, tiled=True)
    return arrived.astype(jnp.float32).sum(axis=0)


def pair_combine(earlier, later):
    return (
        later[0] * earlier[0] - later[1] * earlier[1],
        later[0] * earlier[1] + later[1] * earlier[0],
        later[0] * earlier[2] - later[1] * earlier[3] + later[2],
        later[0] * earlier[3] + later[1] * earlier[2] + later[3],
    )


def block_diagonal(matrix, same_group):
    group_here, inner_size, outer_size = matrix.shape
    spread = matrix[:, :, None, :] * same_group[:, None, :, None]
    return spread.reshape(group_here * inner_size, group_here * outer_size)


def on_device(
    tokens,
    norm_gain,
    w_value,
    w_gate,
    w_drive,
    conv_taps,
    conv_gain,
    log_step,
    step_shift,
    state_real,
    state_imag,
    in_map,
    out_map,
    skip_gain,
    start_state,
    conv_proj,
    state_proj,
):
    row_count = tokens.shape[0]
    tokens_wide = tokens.astype(jnp.float32)
    inverse_rms = lax.rsqrt(jnp.mean(tokens_wide * tokens_wide, axis=1, keepdims=True) + 1e-06)
    normed = (tokens_wide * inverse_rms * norm_gain).astype(jnp.bfloat16)
    conv_width = w_value.shape[1]
    stacked = jnp.concatenate(sent_together((w_value, w_gate, w_drive), SP, 0, 1), axis=1)
    projected = jnp.dot(normed, stacked, preferred_element_type=jnp.float32)
    glu_value = projected[:, :conv_width].astype(jnp.bfloat16)
    glu_gate = projected[:, conv_width : 2 * conv_width].astype(jnp.bfloat16)
    drive_in = projected[:, 2 * conv_width :].astype(jnp.bfloat16)
    gated = (glu_value.astype(jnp.float32) * jax.nn.sigmoid(glu_gate.astype(jnp.float32))).astype(
        jnp.bfloat16
    )
    tap_count = conv_taps.shape[0]
    before = from_behind(gated[row_count - tap_count + 1 :], SP, 1)
    padded = jnp.concatenate([before, gated], axis=0)
    conv_mix = jnp.zeros((row_count, conv_width), jnp.float32)
    for lag_index in range(tap_count):
        conv_mix = conv_mix + conv_taps[lag_index] * padded[
            lag_index : lag_index + row_count
        ].astype(jnp.float32)
    part_sum = jnp.sum(conv_mix, axis=1, keepdims=True)
    part_square = jnp.sum(conv_mix * conv_mix, axis=1, keepdims=True)
    full_sum, full_square = packed_total((part_sum, part_square), "tp")
    channel_count = conv_width * lax.axis_size("tp")
    row_mean = full_sum / channel_count
    row_var = full_square / channel_count - row_mean * row_mean
    conv_out = jax.nn.silu((conv_mix - row_mean) * lax.rsqrt(row_var + 1e-05) * conv_gain).astype(
        jnp.bfloat16
    )
    group_count = state_real.shape[0]
    state_count = state_real.shape[1]
    group_width = in_map.shape[3]
    flat_size = group_count * state_count
    same_group = (jnp.arange(group_count)[:, None] == jnp.arange(group_count)[None, :]).astype(
        jnp.float32
    )
    in_real = block_diagonal(jnp.transpose(in_map[0], (0, 2, 1)), same_group)
    in_imag = block_diagonal(jnp.transpose(in_map[1], (0, 2, 1)), same_group)
    out_real = block_diagonal(jnp.transpose(out_map[0], (0, 2, 1)), same_group)
    out_imag = block_diagonal(jnp.transpose(out_map[1], (0, 2, 1)), same_group)
    rate_re = state_real.reshape(1, flat_size)
    rate_im = state_imag.reshape(1, flat_size)
    rate_size = rate_re * rate_re + rate_im * rate_im
    skip_row = skip_gain.reshape(1, group_count * group_width)
    block_rows = math.gcd(row_count, 128)
    block_count = row_count // block_rows
    steps_all = jnp.exp(log_step[None, :] + step_shift).reshape(
        block_count, block_rows, group_count
    )
    drive_wide = drive_in.astype(jnp.float32)
    drive_all = drive_wide.reshape(block_count, block_rows, group_count * group_width)

    def sweep(state_carry, inputs):
        carry_re, carry_im, prod_re, prod_im = state_carry
        step_block, drive_block = inputs
        step_full = jnp.broadcast_to(
            step_block[:, :, None], (block_rows, group_count, state_count)
        ).reshape(block_rows, flat_size)
        decay_mag = jnp.exp(rate_re * step_full)
        keep_re = decay_mag * jnp.cos(rate_im * step_full)
        keep_im = decay_mag * jnp.sin(rate_im * step_full)
        mapped_re = jnp.dot(drive_block, in_real, precision=lax.Precision.HIGHEST)
        mapped_im = jnp.dot(drive_block, in_imag, precision=lax.Precision.HIGHEST)
        minus_re = keep_re - 1.0
        coeff_re = (minus_re * rate_re + keep_im * rate_im) / rate_size
        coeff_im = (keep_im * rate_re - minus_re * rate_im) / rate_size
        input_re = coeff_re * mapped_re - coeff_im * mapped_im
        input_im = coeff_re * mapped_im + coeff_im * mapped_re
        cum_re, cum_im, local_re, local_im = lax.associative_scan(
            pair_combine, (keep_re, keep_im, input_re, input_im), axis=0
        )
        state_re = local_re + cum_re * carry_re - cum_im * carry_im
        state_im = local_im + cum_re * carry_im + cum_im * carry_re
        full_re = cum_re * prod_re - cum_im * prod_im
        full_im = cum_re * prod_im + cum_im * prod_re
        new_carry = (state_re[-1:], state_im[-1:], full_re[-1:], full_im[-1:])
        return (new_carry, (state_re, state_im, full_re, full_im))

    zero_row = jnp.zeros((1, flat_size), jnp.float32)
    one_row = jnp.ones((1, flat_size), jnp.float32)
    totals, kept = lax.scan(sweep, (zero_row, zero_row, one_row, zero_row), (steps_all, drive_all))
    last_re, last_im, whole_re, whole_im = totals
    prefix_are, prefix_aim, prefix_bre, prefix_bim = carried_in(
        (whole_re, whole_im, last_re, last_im),
        SP,
        pair_combine,
        (one_row, zero_row, zero_row, zero_row),
    )
    first_re = start_state[0].reshape(1, flat_size)
    first_im = start_state[1].reshape(1, flat_size)
    entry_re = prefix_bre + prefix_are * first_re - prefix_aim * first_im
    entry_im = prefix_bim + prefix_are * first_im + prefix_aim * first_re
    own_re = kept[0].reshape(row_count, flat_size)
    own_im = kept[1].reshape(row_count, flat_size)
    span_re = kept[2].reshape(row_count, flat_size)
    span_im = kept[3].reshape(row_count, flat_size)
    state_re = own_re + span_re * entry_re - span_im * entry_im
    state_im = own_im + span_re * entry_im + span_im * entry_re
    ssm_pre = (
        jnp.dot(state_re, out_real, precision=lax.Precision.HIGHEST)
        - jnp.dot(state_im, out_imag, precision=lax.Precision.HIGHEST)
        + skip_row * drive_wide
    )
    ssm_out = jax.nn.gelu(ssm_pre).astype(jnp.bfloat16)
    joined = jnp.concatenate([conv_out, ssm_out], axis=1)
    weights = jnp.concatenate([conv_proj, state_proj], axis=0)
    partial_value = jnp.dot(
        joined, lax.all_gather(weights, SP, axis=1, tiled=True), preferred_element_type=jnp.float32
    )
    return sent_and_summed(partial_value.astype(jnp.bfloat16), "tp", 1).astype(jnp.bfloat16)


def solution(mesh):
    finer = Mesh(mesh.devices.reshape(8, 8, 2, mesh.shape["tp"]), ("sp_0", "sp_1", "sp_2", "tp"))
    placed = (
        P(SP, None),
        P(),
        P(SP, "tp"),
        P(SP, "tp"),
        P(SP, "tp"),
        P(None, "tp"),
        P("tp"),
        P("tp"),
        P(SP, "tp"),
        P("tp", None),
        P("tp", None),
        P(None, "tp", None, None),
        P(None, "tp", None, None),
        P("tp", None),
        P(None, "tp", None),
        P("tp", SP),
        P("tp", SP),
    )
    return jax.shard_map(
        on_device, mesh=finer, in_specs=placed, out_specs=P(SP, "tp"), check_vma=False
    )
```

profile of v0, /device:TPU:1, one launch (start us, length us, event | category | flops | bytes accessed | tf_op | source)
XLA Modules:
  0.0 253.3 jit_solution(8021710322744488060)
XLA Ops:
  6.6 1.4 pad_maximum_fusion.25
  8.1 1.3 pad_maximum_fusion.26
  9.5 1.0 slice_bitcast_fusion.34
  10.5 1.6 slice_bitcast_fusion.33
  12.1 2.1 fusion.16
  14.2 0.6 add_rsqrt_fusion.1
  15.5 0.9 mul.4076
  16.4 0.9 mul.4081
  17.3 0.6 mul.4082
  17.9 0.7 exponential_bitcast_fusion
  18.6 80.8 %all-gather.9.cloned.1.call-done = bf16[2048,384]{1,0:T(8,128)(2,1)} async-done(((bf16[16,384]{1,0:T(8,128)(2,1)}), bf16[2048,384]{1,0:T(8,128)(2,1)}) %all-gather.9.cloned.1.call-update) | async-done | bytes 1572880 | tf_op jit(solution)/shard_map/all_gather | solution.py:15
  99.4 2.7 %fusion.23 = bf16[512,384]{1,0:T(8,128)(2,1)S(1)} fusion(bf16[2048,384]{1,0:T(8,128)(2,1)} %all-gather.9.cloned.1.call-done, bf16[512,2048]{1,0:T(8,128)(2,1)S(1)} %copy-done, f32[2048]{0:T(1024)} %param.20, f32[512]{0:T(512)S(1)} %copy-done.26), kind=kOutput, calls=%fused_computation.179 | convolution fusion | flops 809697280 | bytes 4073472 | tf_op jit(solution)/shard_map/dot_general | solution.py:133
  102.2 0.7 copy-done.6
  103.0 41.7 %while.28 = (s32[]{:T(128)}, f32[1,512]{1,0:T(1,128)S(1)}, f32[1,512]{1,0:T(1,128)S(1)}, f32[1,512]{1,0:T(1,128)S(1)}, f32[1,512]{1,0:T(1,128)S(1)}, /*index=5*/...) while((s32[]{:T(128)}, f32[1,512]{1,0:T(1,128)S(1)}, ...), condition=%wide.region_5.6_spmd.clone.clone, body=%wide.region_4.5_spmd.clone.clone.sunk | while | flops 206416896 | bytes 37394152 | solution.py:208
  103.3 0.4 fusion.130
  104.0 1.5 multiply_add_fusion.48
  109.0 0.2 slice.3012
  109.2 0.2 slice.3013
  111.4 0.8 bitcast_dynamic-update-slice_fusion.6
  112.3 1.1 bitcast_dynamic-update-slice_fusion.7
  113.7 0.4 fusion.130
  114.4 1.5 multiply_add_fusion.48
  121.9 0.8 bitcast_dynamic-update-slice_fusion.6
  122.7 1.0 bitcast_dynamic-update-slice_fusion.7
  124.2 0.4 fusion.130
  124.9 1.5 multiply_add_fusion.48
  132.3 0.8 bitcast_dynamic-update-slice_fusion.6
  133.1 1.1 bitcast_dynamic-update-slice_fusion.7
  134.6 0.4 fusion.130
  135.3 1.5 multiply_add_fusion.48
  142.7 0.8 bitcast_dynamic-update-slice_fusion.6
  143.5 1.1 bitcast_dynamic-update-slice_fusion.7
  144.7 1.9 all-gather.3
  146.7 19.4 %all-gather.4 = f32[8,4,512]{2,1,0:T(4,128)S(1)} all-gather(f32[1,4,512]{2,1,0:T(4,128)S(1)} %maximum_bitcast_fusion.1), channel_id=3, replica_groups=mesh['sp_0'=8,'sp_1'=8,'sp_2'=2,'tp'=4] {'sp_1'}, dimensions={0}, use_global_device_ids=true | all-gather | bytes 73728 | tf_op jit(solution)/shard_map/all_gather | solution.py:57
  166.4 18.6 %all-gather.5 = f32[8,4,512]{2,1,0:T(4,128)S(1)} all-gather(f32[1,4,512]{2,1,0:T(4,128)S(1)} %maximum_bitcast_fusion.2), channel_id=4, replica_groups=mesh['sp_0'=8,'sp_1'=8,'sp_2'=2,'tp'=4] {'sp_0'}, dimensions={0}, use_global_device_ids=true | all-gather | bytes 73728 | tf_op jit(solution)/shard_map/all_gather | solution.py:57
  185.1 1.0 multiply_convert_fusion.1
  186.2 14.1 %collective-permute-start = (bf16[30,128]{1,0:T(8,128)(2,1)S(1)}, bf16[30,128]{1,0:T(8,128)(2,1)S(1)}, u32[]{:S(2)}, u32[]{:S(2)}) collective-permute-start(bf16[30,128]{1,0:T(8,128)(2,1)S(1)} %slice.1834), channel_id=1, source_target_pairs={{0,4},{4,8},{8,12},{12,16},{16,20},{20,24},{24,28},{28,32},{32,36}... | collective-permute-start | bytes 23048 | tf_op jit(solution)/shard_map/ppermute | solution.py:22
  200.6 2.4 multiply_add_fusion.16
  203.0 1.0 fusion.114
  204.1 1.2 fusion.101
  205.3 0.6 broadcast_in_dim.66
  205.9 4.0 %all-to-all-start = ((f32[4,1,1024]{2,1,0:T(1,128)}), f32[4,1,1024]{2,1,0:T(1,128)S(1)}, u32[]{:S(2)}, u32[]{:S(2)}) async-start(f32[4,1,1024]{2,1,0:T(1,128)} %broadcast_in_dim.66), calls=%async_computation | async-start | bytes 32768 | tf_op jit(solution)/shard_map/all_to_all | solution.py:27
  209.9 1.9 fusion.34
  211.8 2.3 all-to-all-done
  214.2 0.2 multiply_convert_fusion
  214.4 2.0 convolution_convert_fusion
  216.6 28.6 %all_to_all.11 = bf16[4,512,512]{2,1,0:T(8,128)(2,1)S(1)} all-to-all(bf16[4,512,512]{2,1,0:T(8,128)(2,1)S(1)} %bitcast.671), channel_id=1, replica_groups=mesh['sp_0'=8,'sp_1'=8,'sp_2'=2,'tp'=4] {'tp'}, dimensions={0} | all-to-all | bytes 4194304 | tf_op jit(solution)/shard_map/all_to_all | solution.py:89
  245.2 1.2 reduce_sum.52
  (981 shorter events, 23.1 us)
Async XLA Ops:
  6.5 8.3 %copy-start.11 = (f32[8,64]{1,0:T(8,128)S(1)}, f32[8,64]{1,0:T(8,128)}, u32[]{:S(2)}) copy-start(f32[8,64]{1,0:T(8,128)} %param.28) | copy-start | bytes 6148
  6.5 8.4 %copy-start.12 = (f32[8,64]{1,0:T(8,128)S(1)}, f32[8,64]{1,0:T(8,128)}, u32[]{:S(2)}) copy-start(f32[8,64]{1,0:T(8,128)} %param.29) | copy-start | bytes 6148
  6.5 8.4 %copy-start.7 = (f32[2,8,64,16]{2,3,1,0:T(8,128)S(1)}, f32[2,8,64,16]{2,3,1,0:T(8,128)}, u32[]{:S(2)}) copy-start(f32[2,8,64,16]{2,3,1,0:T(8,128)} %param.30) | copy-start | bytes 196612
  6.5 8.4 %copy-start.10 = (f32[2,8,64]{2,1,0:T(8,128)S(1)}, f32[2,8,64]{2,1,0:T(8,128)}, u32[]{:S(2)}) copy-start(f32[2,8,64]{2,1,0:T(8,128)} %param.33) | copy-start | bytes 12292
  6.5 8.6 %copy-start.8 = (f32[2,8,16,64]{3,2,1,0:T(8,128)S(1)}, f32[2,8,16,64]{3,2,1,0:T(8,128)}, u32[]{:S(2)}) copy-start(f32[2,8,16,64]{3,2,1,0:T(8,128)} %param.31) | copy-start | bytes 196612
  6.5 92.9 %all-gather.9.cloned.1.call-start = ((), (), s32[]{:S(2)}) async-start(), calls=%async_computation.2 | async-start | bytes 1585152 | tf_op jit(solution)/shard_map/all_gather | solution.py:15
  8.1 206.4 %all-gather.11.cloned.1.call-start = ((), (), s32[]{:S(2)}) async-start(), calls=%async_computation.3 | async-start | bytes 1056768 | tf_op jit(solution)/shard_map/all_gather | solution.py:235
  14.2 3.1 %copy-start.13 = (f32[8,16]{1,0:T(8,128)S(1)}, f32[8,16]{1,0:T(8,128)}, u32[]{:S(2)}) copy-start(f32[8,16]{1,0:T(8,128)} %param.32) | copy-start | bytes 1540
  14.2 3.7 %copy-start.9 = (f32[512,8]{0,1:T(8,128)S(1)}, f32[512,8]{0,1:T(8,128)}, u32[]{:S(2)}) copy-start(f32[512,8]{0,1:T(8,128)} %param.27) | copy-start | bytes 49156
  14.2 85.2 %copy-start = (bf16[512,2048]{1,0:T(8,128)(2,1)S(1)}, bf16[512,2048]{1,0:T(8,128)(2,1)}, u32[]{:S(2)}) copy-start(bf16[512,2048]{1,0:T(8,128)(2,1)} %param.19) | copy-start | bytes 6291460
  15.0 84.4 %copy-start.26 = (f32[512]{0:T(512)S(1)}, f32[512]{0:T(512)}, u32[]{:S(2)}) copy-start(f32[512]{0:T(512)} %add_rsqrt_fusion.1) | copy-start | bytes 6148
  102.1 0.7 copy-start.6
  103.0 2.5 copy-start.1
  103.0 2.5 copy-start.24
  112.3 1.1 copy-start.2
  112.3 1.1 copy-start.25
  113.4 2.5 copy-start.1
  113.4 2.5 copy-start.24
  122.7 1.1 copy-start.2
  122.7 1.1 copy-start.25
  123.8 2.5 copy-start.1
  123.8 2.5 copy-start.24
  133.1 1.1 copy-start.2
  133.1 1.1 copy-start.25
  134.2 2.5 copy-start.1
  134.3 2.5 copy-start.24
  143.5 1.1 copy-start.2
  143.5 1.1 copy-start.25
  144.7 55.8 %copy-start.5 = (f32[4,128,512]{2,1,0:T(8,128)S(1)}, f32[4,128,512]{2,1,0:T(8,128)}, u32[]{:S(2)}) copy-start(f32[4,128,512]{2,1,0:T(8,128)} %get-tuple-element.209) | copy-start | bytes 3145732
  186.2 17.8 %collective-permute-start = (bf16[30,128]{1,0:T(8,128)(2,1)S(1)}, bf16[30,128]{1,0:T(8,128)(2,1)S(1)}, u32[]{:S(2)}, u32[]{:S(2)}) collective-permute-start(bf16[30,128]{1,0:T(8,128)(2,1)S(1)} %slice.1834), channel_id=1, source_target_pairs={{0,4},{4,8},{8,12},{12,16},{16,20},{20,24},{24,28},{28,32},{32,36}... | collective-permute-start | bytes 23048 | tf_op jit(solution)/shard_map/ppermute | solution.py:22
  200.5 2.5 copy-start.4
  200.5 3.5 %copy-start.14 = (f32[128]{0:T(128)S(1)}, f32[128]{0:T(128)}, u32[]{:S(2)}) copy-start(f32[128]{0:T(128)} %get-tuple-element.562) | copy-start | bytes 1540
  200.5 3.5 %copy-start.15 = (f32[128]{0:T(128)S(1)}, f32[128]{0:T(128)}, u32[]{:S(2)}) copy-start(f32[128]{0:T(128)} %get-tuple-element.563) | copy-start | bytes 1540
  200.5 3.5 %copy-start.16 = (f32[128]{0:T(128)S(1)}, f32[128]{0:T(128)}, u32[]{:S(2)}) copy-start(f32[128]{0:T(128)} %get-tuple-element.564) | copy-start | bytes 1540
  200.5 3.5 %copy-start.17 = (f32[128]{0:T(128)S(1)}, f32[128]{0:T(128)}, u32[]{:S(2)}) copy-start(f32[128]{0:T(128)} %get-tuple-element.565) | copy-start | bytes 1540
  200.5 3.5 %copy-start.18 = (f32[128]{0:T(128)S(1)}, f32[128]{0:T(128)}, u32[]{:S(2)}) copy-start(f32[128]{0:T(128)} %get-tuple-element.566) | copy-start | bytes 1540
  200.5 3.5 %copy-start.19 = (f32[128]{0:T(128)S(1)}, f32[128]{0:T(128)}, u32[]{:S(2)}) copy-start(f32[128]{0:T(128)} %get-tuple-element.567) | copy-start | bytes 1540
  200.5 3.5 %copy-start.20 = (f32[128]{0:T(128)S(1)}, f32[128]{0:T(128)}, u32[]{:S(2)}) copy-start(f32[128]{0:T(128)} %get-tuple-element.568) | copy-start | bytes 1540
  200.5 3.5 %copy-start.21 = (f32[128]{0:T(128)S(1)}, f32[128]{0:T(128)}, u32[]{:S(2)}) copy-start(f32[128]{0:T(128)} %get-tuple-element.569) | copy-start | bytes 1540
  200.6 3.5 %copy-start.22 = (f32[128]{0:T(128)S(1)}, f32[128]{0:T(128)}, u32[]{:S(2)}) copy-start(f32[128]{0:T(128)} %get-tuple-element.570) | copy-start | bytes 1540
  200.6 3.5 %copy-start.23 = (f32[128]{0:T(128)S(1)}, f32[128]{0:T(128)}, u32[]{:S(2)}) copy-start(f32[128]{0:T(128)} %get-tuple-element.571) | copy-start | bytes 1540
  203.0 7.0 %copy-start.3 = (f32[512,128]{0,1:T(8,128)S(1)}, f32[512,128]{0,1:T(8,128)}, u32[]{:S(2)}) copy-start(f32[512,128]{0,1:T(8,128)} %mul.4081) | copy-start | bytes 786436
  203.0 6.9 %copy-start.27 = (f32[128]{0:T(128)S(1)}, f32[128]{0:T(128)}, u32[]{:S(2)}) copy-start(f32[128]{0:T(128)} %mul.4082) | copy-start | bytes 1540
  203.0 11.2 %copy-start.28 = (f32[128]{0:T(128)S(1)}, f32[128]{0:T(128)}, u32[]{:S(2)}) copy-start(f32[128]{0:T(128)} %param.25) | copy-start | bytes 1540
  205.9 8.2 %all-to-all-start = ((f32[4,1,1024]{2,1,0:T(1,128)}), f32[4,1,1024]{2,1,0:T(1,128)S(1)}, u32[]{:S(2)}, u32[]{:S(2)}) async-start(f32[4,1,1024]{2,1,0:T(1,128)} %broadcast_in_dim.66), calls=%async_computation | async-start | bytes 32768 | tf_op jit(solution)/shard_map/all_to_all | solution.py:27
Sparse Core Ops, SparseCore 0:
  10.6 88.8 all-gather.8
  102.4 76.1 all-gather.10
where the time goes:
time: 254 us; the launch traced here: 253 us
  waiting for transfers between devices  83.2 us (33%)
  blocking collectives  68.6 us (27%)
  other arithmetic  25.4 us (10%)
  local copies, waits for them, and re-layouts  24 us (9%)
  starting transfers between devices  18.1 us (7%)
  matrix products  14.9 us (6%)
  between operations  14.1 us (6%)
  loops' own time  5.06 us (2%)
    all_gather x1, waiting for transfers between devices, sent_together(): out = lax.all_gather(both, axis, axis=dim, tiled=True)  80.8 us
    all_gather x3, blocking collectives, gathered_once(): both, at, found = (lax.all_gather(jnp.concatenate(lines), axis), 0, {})  40 us
    all_to_all x1, blocking collectives, sent_and_summed(): lax.all_to_all(pieces, axis, split_axis=0, concat_axis=0, tiled=True)  28.6 us
    ppermute x1, starting transfers between devices, from_behind(): return lax.ppermute(x, axis, pairs)  14.1 us
    slice x364, local copies, waits for them, and re-layouts, sweep(): lax.associative_scan(pair_combine, (keep_re, keep_im, input_re, input_im)...  11.6 us
    dynamic_update_slice x8, other arithmetic, on_device(): lax.scan(sweep, (zero_row, zero_row, one_row, zero_row), (steps_all, driv...  7.57 us
    dot_general x4, matrix products, sweep(): mapped_re = jnp.dot(drive_block, in_real, precision=lax.Precision.HIGHEST)  5.82 us
  transfers between devices with their start and end apart: 4, of which 2 were waited for; matrix products, arithmetic and copies ran while one was open for 23% of the time, Pallas kernels for 0%

commit v1 on v0

v1 whole, which is shorter than its diff:
```python
import functools
import math

import jax
import jax.numpy as jnp
from jax import lax
from jax.experimental import pallas as pl
from jax.experimental.pallas import tpu as pltpu
from jax.sharding import PartitionSpec as P

MESH = pl.DeviceIdType.MESH
F32, BF16 = jnp.float32, jnp.bfloat16
HIGHEST = lax.Precision.HIGHEST
CHUNKS = 8
LANES = 128
PI_HEAD, PI_MID, PI_TAIL = 3.140625, 9.67502593994140625e-4, 1.509957990978376432e-7
SIN = (
    0.9999999956945582,
    -0.16666657935421791,
    0.008333049779224343,
    -0.00019808982983932522,
    2.605019582042587e-06,
)
COS = (
    0.9999999997785899,
    -0.4999999935376166,
    0.04166663608814349,
    -0.0013888359276841241,
    2.476005397141232e-05,
    -2.6049608226484117e-07,
)


def series(terms, x):
    total = terms[-1]
    for term in reversed(terms[:-1]):
        total = total * x + term
    return total


def keep_of(rate_re, rate_im, step):
    angle = rate_im * step
    turns = jnp.floor(angle * (1.0 / math.pi) + 0.5)
    rest = ((angle - turns * PI_HEAD) - turns * PI_MID) - turns * PI_TAIL
    square = rest * rest
    half = turns * 0.5
    size = jnp.exp(rate_re * step) * (1.0 - 4.0 * (half - jnp.floor(half)))
    return size * series(COS, square), size * (rest * series(SIN, square))


def nn(a, b, precision=None):
    return lax.dot_general(
        a, b, (((1,), (0,)), ((), ())), precision=precision, preferred_element_type=F32
    )


def nt(a, b, precision=None):
    return lax.dot_general(
        a, b, (((1,), (1,)), ((), ())), precision=precision, preferred_element_type=F32
    )


def tn(a, b, precision=None):
    return lax.dot_general(
        a, b, (((0,), (0,)), ((), ())), precision=precision, preferred_element_type=F32
    )


def ids(shape, dim):
    return lax.broadcasted_iota(jnp.int32, shape, dim)


def split_two(x):
    head = x.astype(BF16)
    return head, (x - head.astype(F32)).astype(BF16)


def entry_of(arrived, side, place, rate_re, rate_im, q):
    real = arrived[pl.ds(q, side, stride=16), :]
    imag = arrived[pl.ds(4 + q, side, stride=16), :]
    step = arrived[pl.ds(8 + q, side, stride=16), :]
    row = ids((side, LANES), 0)
    since = jnp.zeros((side, LANES), F32)
    for k in range(side):
        since = since + jnp.where((row < k) & (place > k), step[k : k + 1], 0.0)
    turn_re, turn_im = keep_of(rate_re, rate_im, since)
    before = row < place
    got_re = jnp.where(before, turn_re * real - turn_im * imag, 0.0)
    got_im = jnp.where(before, turn_re * imag + turn_im * real, 0.0)
    ahead = jnp.where(before, step, 0.0)
    return (
        jnp.sum(got_re, axis=0, keepdims=True),
        jnp.sum(got_im, axis=0, keepdims=True),
        jnp.sum(ahead, axis=0, keepdims=True),
    )


def kernel(
    dims,
    tokens_hbm,
    value_hbm,
    gate_hbm,
    drive_hbm,
    convp_hbm,
    statep_hbm,
    gain_ref,
    taps_ref,
    conv_gain_ref,
    log_step_ref,
    shift_ref,
    rate_re_ref,
    rate_im_ref,
    in_ref,
    out_map_ref,
    skip_ref,
    start_ref,
    out_ref,
    tok,
    nrm,
    gd,
    gv,
    pz,
    py,
    wd,
    wvg,
    wo,
    dtx,
    kr,
    ki,
    cr,
    ci,
    mr,
    mi,
    in_blocks,
    out_blocks,
    drv,
    drvp,
    gf,
    cm,
    halo,
    halo_send,
    st_send,
    st_recv,
    mc_send,
    mc_recv,
    my_all,
    mz_all,
    act,
    local_sem,
    d1s,
    d1r,
    v1s,
    v1r,
    p1s,
    p1r,
    d2s,
    d2r,
    v2s,
    v2r,
    p2s,
    p2r,
    p3s,
    p3r,
    dcs,
    dcr,
    vcs,
    vcr,
    pcs,
    pcr,
    misc_s,
    misc_r,
    cys,
    cyr,
    czs,
    czr,
    sts,
    strv,
    acs,
    acr,
    ass,
    asr,
):
    side, cols = dims
    rows, depth = tokens_hbm.shape
    planes = side // cols
    sp, x = lax.axis_index("sp"), lax.axis_index("tp")
    c = lax.rem(sp, 2)
    chip = lax.div(sp, 2)
    y, z = lax.rem(chip, side), lax.div(chip, side)
    count = 2 * side * side
    steps = rows // CHUNKS

    def at(zz, yy, cc):
        return (zz * side + yy) * 2 + cc

    def turn(a, k):
        return lax.rem(a + k, side)

    mate = at(z, y, 1 - c)
    b_me, a_me = c * z + (1 - c) * y, c * y + (1 - c) * z

    def b_peer(b):
        return c * at(b, y, 1) + (1 - c) * at(z, b, 0)

    def a_peer(a):
        return c * at(z, a, 1) + (1 - c) * at(a, y, 0)

    beyond = lax.rem(sp + 2 * c - 1 + count, count)
    following = lax.rem(sp + 1, count)

    def copy(src, dst, send_sem, recv_sem, to_sp, to_x):
        return pltpu.make_async_remote_copy(
            src_ref=src,
            dst_ref=dst,
            send_sem=send_sem,
            recv_sem=recv_sem,
            device_id=(to_sp, to_x),
            device_id_type=MESH,
        )

    sent = []

    def send(*args):
        one = copy(*args)
        one.start()
        sent.append(one)

    def arrive(dst, send_sem, recv_sem):
        copy(dst, dst, send_sem, recv_sem, mate, x).wait_recv()

    own_copies = [
        pltpu.make_async_copy(drive_hbm, gd.at[c, a_me, b_me], local_sem.at[0]),
        pltpu.make_async_copy(value_hbm, gv.at[c, a_me, b_me, :, pl.ds(0, LANES)], local_sem.at[1]),
        pltpu.make_async_copy(gate_hbm, gv.at[c, a_me, b_me, :, pl.ds(LANES, LANES)], local_sem.at[2]),
        pltpu.make_async_copy(convp_hbm, pz.at[z, :, pl.ds(0, LANES)], local_sem.at[3]),
        pltpu.make_async_copy(statep_hbm, pz.at[z, :, pl.ds(LANES, LANES)], local_sem.at[4]),
        pltpu.make_async_copy(tokens_hbm, tok, local_sem.at[5]),
    ]
    for one in own_copies:
        one.start()

    barrier = pltpu.get_barrier_semaphore()

    def greet(to_sp, to_x):
        pl.semaphore_signal(barrier, inc=1, device_id=(to_sp, to_x), device_id_type=MESH)

    greet(mate, x)
    greet(beyond, x)
    for k in range(1, side):
        greet(at(z, turn(y, k), c), x)
        greet(at(turn(z, k), y, c), x)
    for k in range(1, cols):
        greet(sp, lax.rem(x + k, cols))

    wide = 4 * LANES
    group_mask = (ids((LANES, wide), 1) // 64 == ids((LANES, wide), 0) // 16).astype(F32)
    spread = (ids((64, wide), 1) % 64 == ids((64, wide), 0)).astype(F32)
    for half in range(2):
        part = pl.ds(half * LANES, LANES)
        tiled = nn(in_ref[part, :], spread, HIGHEST) * group_mask
        head, tail = split_two(tiled)
        in_blocks[half, 0], in_blocks[half, 1] = head, tail
        tiled = nn(out_map_ref[part, :], spread, HIGHEST) * group_mask
        head, tail = split_two(tiled)
        out_blocks[half, 0], out_blocks[half, 1] = head, tail
    own_group = (ids((8, wide), 1) // 64 == ids((8, wide), 0)).astype(F32)

    def flat(value):
        return jnp.sum(nn(value, spread, HIGHEST) * own_group, axis=0, keepdims=True)

    rate_re, rate_im = flat(rate_re_ref[...]), flat(rate_im_ref[...])
    first_re, first_im = flat(start_ref[0:8, :]), flat(start_ref[8:16, :])
    size = rate_re * rate_re + rate_im * rate_im
    inv_re, inv_im = rate_re / size, rate_im / size
    spread16 = (ids((16, LANES), 1) % 16 == ids((16, LANES), 0)).astype(F32)
    own16 = (ids((8, LANES), 1) // 16 == ids((8, LANES), 0)).astype(F32)
    skip_row = jnp.sum(nn(skip_ref[...], spread16, HIGHEST) * own16, axis=0, keepdims=True)
    eye8 = ids((8, 8), 0) == ids((8, 8), 1)
    log_step = jnp.sum(jnp.where(eye8, log_step_ref[...], 0.0), axis=1, keepdims=True)
    dt = jnp.exp(log_step + shift_ref[...])

    def tile(v, q):
        return v[:, q * LANES : (q + 1) * LANES]

    for q in range(4):
        dtx[q] = tn(dt, tile(own_group, q), HIGHEST)

    pl.semaphore_wait(barrier, 2 * side + cols - 1)
    for one in own_copies[:5]:
        one.wait()
    for k in range(1, side):
        here = gd.at[c, a_me, b_me]
        send(here, here, d1s.at[k], d1r.at[k], b_peer(turn(b_me, k)), x)
    for k in range(1, side):
        here = gv.at[c, a_me, b_me]
        send(here, here, v1s.at[k], v1r.at[k], b_peer(turn(b_me, k)), x)
    for k in range(1, side):
        here = pz.at[z]
        send(here, here, p1s.at[k], p1r.at[k], at(turn(z, k), y, c), x)

    own_copies[5].wait()
    gain = gain_ref[...]

    def norm_rows(i, carry):
        r = pl.ds(pl.multiple_of(i * 16, 16), 16)
        wide_rows = tok[r, :].astype(F32)
        mean = jnp.sum(wide_rows * wide_rows, axis=1, keepdims=True) * (1.0 / depth)
        nrm[r, :] = (wide_rows * lax.rsqrt(mean + 1e-06) * gain).astype(BF16)
        return carry

    lax.fori_loop(0, rows // 16, norm_rows, 0)

    for k in range(1, side):
        arrive(gd.at[c, a_me, turn(b_me, side - k)], d1s.at[k], d1r.at[k])
    line = gd.at[c, a_me]
    for k in range(1, side):
        send(line, line, d2s.at[k], d2r.at[k], a_peer(turn(a_me, k)), x)
    send(line, line, dcs.at[0], dcr.at[0], mate, x)
    for k in range(1, side):
        arrive(gv.at[c, a_me, turn(b_me, side - k)], v1s.at[k], v1r.at[k])
    line = gv.at[c, a_me]
    for k in range(1, side):
        send(line, line, v2s.at[k], v2r.at[k], a_peer(turn(a_me, k)), x)
    send(line, line, vcs.at[0], vcr.at[0], mate, x)
    for k in range(1, side):
        arrive(pz.at[turn(z, side - k)], p1s.at[k], p1r.at[k])
    for k in range(1, cols):
        to = lax.rem(x + k, cols)
        send(pz.at[pl.ds(to * planes, planes)], py.at[c, y, x], p2s.at[k], p2r.at[k], sp, to)
    py[c, y, x] = pz[pl.ds(x * planes, planes)]

    def keep_rows(j, carry):
        r = pl.ds(pl.multiple_of(j * 8, 8), 8)
        new = []
        for q in range(4):
            step = dtx[q, pl.ds(j, CHUNKS, stride=steps), :]
            keep_re, keep_im = keep_of(tile(rate_re, q), tile(rate_im, q), step)
            minus = keep_re - 1.0
            cols_q = pl.ds(q * LANES, LANES)
            kr[r, cols_q] = keep_re
            ki[r, cols_q] = keep_im
            cr[r, cols_q] = minus * tile(inv_re, q) + keep_im * tile(inv_im, q)
            ci[r, cols_q] = keep_im * tile(inv_re, q) - minus * tile(inv_im, q)
            new.append(carry[q] + step)
        return tuple(new)

    zero = jnp.zeros((CHUNKS, LANES), F32)
    spans = lax.fori_loop(0, steps, keep_rows, (zero,) * 4)

    for k in range(1, side):
        block = gd.at[c, turn(a_me, side - k)]
        arrive(block, d2s.at[k], d2r.at[k])
        send(block, block, dcs.at[k], dcr.at[k], mate, x)
    for k in range(side):
        arrive(gd.at[1 - c, turn(b_me, side - k)], dcs.at[k], dcr.at[k])

    def place_drive(a, carry):
        for b in range(side):
            r = pl.multiple_of(at(a, b, 0) * 16, 16)
            wd[pl.ds(r, 16), :] = gd[0, a, b]
            r = pl.multiple_of(at(b, a, 1) * 16, 16)
            wd[pl.ds(r, 16), :] = gd[1, a, b]
        return carry

    lax.fori_loop(0, side, place_drive, 0)
    block_rows = min(rows, 128)

    def drive_rows(i, carry):
        r = pl.ds(pl.multiple_of(i * block_rows, block_rows), block_rows)
        drv[r, :] = nn(nrm[r, :], wd[...]).astype(BF16).astype(F32)
        return carry

    lax.fori_loop(0, rows // block_rows, drive_rows, 0)

    def turn_rows(j, carry):
        r = pl.ds(pl.multiple_of(j * 8, 8), 8)
        drvp[r, :] = drv[pl.ds(j, CHUNKS, stride=steps), :]
        return carry

    lax.fori_loop(0, steps, turn_rows, 0)

    def map_rows(i, carry):
        r = pl.ds(pl.multiple_of(i * block_rows, block_rows), block_rows)
        d = drvp[r, :].astype(BF16)
        mr[r, :] = nn(d, in_blocks[0, 0]) + nn(d, in_blocks[0, 1])
        mi[r, :] = nn(d, in_blocks[1, 0]) + nn(d, in_blocks[1, 1])
        return carry

    lax.fori_loop(0, rows // block_rows, map_rows, 0)

    def scan_rows(j, carry):
        r = pl.ds(pl.multiple_of(j * 8, 8), 8)
        new = []
        for q in range(4):
            cols_q = pl.ds(q * LANES, LANES)
            s_re, s_im = carry[2 * q], carry[2 * q + 1]
            c_re, c_im = cr[r, cols_q], ci[r, cols_q]
            m_re, m_im = mr[r, cols_q], mi[r, cols_q]
            u_re = c_re * m_re - c_im * m_im
            u_im = c_re * m_im + c_im * m_re
            cr[r, cols_q] = u_re
            ci[r, cols_q] = u_im
            k_re, k_im = kr[r, cols_q], ki[r, cols_q]
            new.append((k_re * s_re + u_re) - k_im * s_im)
            new.append((k_re * s_im + u_im) + k_im * s_re)
        return tuple(new)

    finals = lax.fori_loop(0, steps, scan_rows, (zero,) * 8)

    row8 = ids((CHUNKS, LANES), 0)
    starts, mine, ahead_spans = [], [], []
    for q in range(4):
        re_q, im_q = tile(rate_re, q), tile(rate_im, q)
        hop_re, hop_im = keep_of(re_q, im_q, spans[q])
        f_re, f_im = finals[2 * q], finals[2 * q + 1]
        e_re = e_im = total = jnp.zeros((1, LANES), F32)
        l_re = l_im = ahead = zero
        for s in range(CHUNKS):
            l_re = jnp.where(row8 == s, e_re, l_re)
            l_im = jnp.where(row8 == s, e_im, l_im)
            ahead = jnp.where(row8 == s, total, ahead)
            h_re, h_im = hop_re[s : s + 1], hop_im[s : s + 1]
            e_re, e_im = (
                h_re * e_re - h_im * e_im + f_re[s : s + 1],
                h_re * e_im + h_im * e_re + f_im[s : s + 1],
            )
            total = total + spans[q][s : s + 1]
        starts.append((l_re, l_im))
        ahead_spans.append(ahead)
        mine.append((e_re, e_im, total))
        mc_send[q : q + 1, :] = e_re
        mc_send[4 + q : 5 + q, :] = e_im
        mc_send[8 + q : 9 + q, :] = total
    mc_send[12:16, :] = jnp.zeros((4, LANES), F32)
    send(mc_send, mc_recv, misc_s.at[0], misc_r.at[0], mate, x)

    for k in range(1, side):
        block = gv.at[c, turn(a_me, side - k)]
        arrive(block, v2s.at[k], v2r.at[k])
        send(block, block, vcs.at[k], vcr.at[k], mate, x)

    arrive(mc_recv, misc_s.at[0], misc_r.at[0])
    core_entry = []
    second = c == 1
    slot = pl.multiple_of(y * 16, 16)
    for q in range(4):
        re_q, im_q = tile(rate_re, q), tile(rate_im, q)
        m_re, m_im, m_span = mine[q]
        o_re, o_im = mc_recv[q : q + 1, :], mc_recv[4 + q : 5 + q, :]
        o_span = mc_recv[8 + q : 9 + q, :]
        a_re, a_im = jnp.where(second, o_re, m_re), jnp.where(second, o_im, m_im)
        b_re, b_im = jnp.where(second, m_re, o_re), jnp.where(second, m_im, o_im)
        h_re, h_im = keep_of(re_q, im_q, jnp.where(second, m_span, o_span))
        my_all[pl.ds(slot + q, 1), :] = h_re * a_re - h_im * a_im + b_re
        my_all[pl.ds(slot + 4 + q, 1), :] = h_re * a_im + h_im * a_re + b_im
        my_all[pl.ds(slot + 8 + q, 1), :] = m_span + o_span
        none = jnp.zeros_like(o_re)
        core_entry.append(
            (
                jnp.where(second, o_re, none),
                jnp.where(second, o_im, none),
                jnp.where(second, o_span, none),
            )
        )
    my_all[pl.ds(slot + 12, 4), :] = jnp.zeros((4, LANES), F32)
    here = my_all.at[pl.ds(slot, 16), :]
    for k in range(1, side):
        send(here, here, cys.at[k], cyr.at[k], at(z, turn(y, k), c), x)

    for k in range(side):
        arrive(gv.at[1 - c, turn(b_me, side - k)], vcs.at[k], vcr.at[k])

    def place_value(a, carry):
        for b in range(side):
            r = pl.multiple_of(at(a, b, 0) * 16, 16)
            wvg[pl.ds(r, 16), :] = gv[0, a, b]
            r = pl.multiple_of(at(b, a, 1) * 16, 16)
            wvg[pl.ds(r, 16), :] = gv[1, a, b]
        return carry

    lax.fori_loop(0, side, place_value, 0)

    def gate_rows(i, carry):
        i = rows // block_rows - 1 - i
        base = pl.multiple_of(i * block_rows, block_rows)
        both = nn(nrm[pl.ds(base, block_rows), :], wvg[...]).astype(BF16).astype(F32)
        gated = (both[:, :LANES] * jax.nn.sigmoid(both[:, LANES:])).astype(BF16)
        gf[pl.ds(base + 32, block_rows), :] = gated.astype(F32)
        return carry

    lax.fori_loop(0, rows // block_rows, gate_rows, 0)
    halo_send[...] = gf[rows : rows + 32, :].astype(BF16)
    send(halo_send, halo, misc_s.at[1], misc_r.at[1], following, x)

    for k in range(1, side):
        from_y = turn(y, side - k)
        arrive(my_all.at[pl.ds(pl.multiple_of(from_y * 16, 16), 16), :], cys.at[k], cyr.at[k])
    chip_entry = []
    slot_z = pl.multiple_of(z * 16, 16)
    for q in range(4):
        re_q, im_q = tile(rate_re, q), tile(rate_im, q)
        chip_entry.append(entry_of(my_all, side, y, re_q, im_q, q))
        all_re, all_im, all_span = entry_of(my_all, side, side, re_q, im_q, q)
        mz_all[pl.ds(slot_z + q, 1), :] = all_re
        mz_all[pl.ds(slot_z + 4 + q, 1), :] = all_im
        mz_all[pl.ds(slot_z + 8 + q, 1), :] = all_span
    mz_all[pl.ds(slot_z + 12, 4), :] = jnp.zeros((4, LANES), F32)
    here = mz_all.at[pl.ds(slot_z, 16), :]
    for k in range(1, side):
        send(here, here, czs.at[k], czr.at[k], at(turn(z, k), y, c), x)

    arrive(halo, misc_s.at[1], misc_r.at[1])
    gf[0:32, :] = jnp.where(sp == 0, 0.0, halo[...].astype(F32))
    taps = taps_ref.shape[0]
    conv_rows = min(rows, 64)

    def conv_block(i, carry):
        base = pl.multiple_of(i * conv_rows, conv_rows)
        total = jnp.zeros((conv_rows, LANES), F32)
        for k in range(taps):
            total = total + taps_ref[k : k + 1, :] * gf[pl.ds(base + (33 - taps) + k, conv_rows), :]
        cm[pl.ds(base, conv_rows), :] = total
        return carry

    lax.fori_loop(0, rows // conv_rows, conv_block, 0)
    mix = cm[...]
    ones = jnp.ones((8, LANES), F32)
    row_st = ids((8, rows), 0)
    sums = nt(ones, mix, HIGHEST)
    squares = nt(ones, mix * mix, HIGHEST)
    st_send[...] = jnp.where(row_st == 0, sums, jnp.where(row_st == 1, squares, 0.0))
    for k in range(1, cols):
        send(st_send, st_recv.at[k - 1], sts.at[k], strv.at[k], sp, lax.rem(x + k, cols))

    for k in range(1, cols):
        arrive(py.at[c, y, lax.rem(x + cols - k, cols)], p2s.at[k], p2r.at[k])
    line = py.at[c, y]
    for k in range(1, side):
        send(line, line, p3s.at[k], p3r.at[k], at(z, turn(y, k), c), x)
    send(line, line, pcs.at[0], pcr.at[0], mate, x)

    stats = st_send[...]
    for k in range(1, cols):
        arrive(st_recv.at[k - 1], sts.at[k], strv.at[k])
        stats = stats + st_recv[k - 1]
    stats = stats * (1.0 / (cols * LANES))
    pick = ids((8, LANES), 0)
    mean = tn(stats, (pick == 0).astype(F32), HIGHEST)
    square = tn(stats, (pick == 1).astype(F32), HIGHEST)
    scaled = (cm[...] - mean) * lax.rsqrt(square - mean * mean + 1e-05) * conv_gain_ref[...]
    act[x, :, pl.ds(0, LANES)] = (scaled * jax.nn.sigmoid(scaled)).astype(BF16)
    here = act.at[x, :, pl.ds(0, LANES)]
    for k in range(1, cols):
        send(here, here, acs.at[k], acr.at[k], sp, lax.rem(x + k, cols))

    for k in range(1, side):
        from_z = turn(z, side - k)
        arrive(mz_all.at[pl.ds(pl.multiple_of(from_z * 16, 16), 16), :], czs.at[k], czr.at[k])
    begin = []
    for q in range(4):
        re_q, im_q = tile(rate_re, q), tile(rate_im, q)
        s_re, s_im = tile(first_re, q), tile(first_im, q)
        for more_re, more_im, span in (
            entry_of(mz_all, side, z, re_q, im_q, q),
            chip_entry[q],
            core_entry[q],
        ):
            h_re, h_im = keep_of(re_q, im_q, span)
            s_re, s_im = h_re * s_re - h_im * s_im + more_re, h_re * s_im + h_im * s_re + more_im
        h_re, h_im = keep_of(re_q, im_q, ahead_spans[q])
        begin.append(h_re * s_re - h_im * s_im + starts[q][0])
        begin.append(h_re * s_im + h_im * s_re + starts[q][1])

    def state_rows(j, carry):
        r = pl.ds(pl.multiple_of(j * 8, 8), 8)
        new = []
        for q in range(4):
            cols_q = pl.ds(q * LANES, LANES)
            s_re, s_im = carry[2 * q], carry[2 * q + 1]
            k_re, k_im = kr[r, cols_q], ki[r, cols_q]
            n_re = (k_re * s_re + cr[r, cols_q]) - k_im * s_im
            n_im = (k_re * s_im + ci[r, cols_q]) + k_im * s_re
            mr[r, cols_q] = n_re
            mi[r, cols_q] = n_im
            new.extend((n_re, n_im))
        return tuple(new)

    lax.fori_loop(0, steps, state_rows, tuple(begin))

    def read_rows(i, carry):
        r = pl.ds(pl.multiple_of(i * block_rows, block_rows), block_rows)
        re_head, re_tail = split_two(mr[r, :])
        im_head, im_tail = split_two(mi[r, :])
        total = nt(re_head, out_blocks[0, 0]) - nt(im_head, out_blocks[1, 0])
        total = total + (nt(re_tail, out_blocks[0, 0]) - nt(im_tail, out_blocks[1, 0]))
        total = total + (nt(re_head, out_blocks[0, 1]) - nt(im_head, out_blocks[1, 1]))
        drvp[r, :] = jax.nn.gelu(total + skip_row * drvp[r, :])
        return carry

    lax.fori_loop(0, rows // block_rows, read_rows, 0)

    def back_rows(j, carry):
        r = pl.ds(pl.multiple_of(j * 8, 8), 8)
        drv[pl.ds(j, CHUNKS, stride=steps), :] = drvp[r, :]
        return carry

    lax.fori_loop(0, steps, back_rows, 0)
    act[x, :, pl.ds(LANES, LANES)] = drv[...].astype(BF16)
    here = act.at[x, :, pl.ds(LANES, LANES)]
    for k in range(1, cols):
        send(here, here, ass.at[k], asr.at[k], sp, lax.rem(x + k, cols))

    for k in range(1, side):
        block = py.at[c, turn(y, side - k)]
        arrive(block, p3s.at[k], p3r.at[k])
        send(block, block, pcs.at[k], pcr.at[k], mate, x)
    for k in range(side):
        arrive(py.at[1 - c, turn(y, side - k)], pcs.at[k], pcr.at[k])

    def place_out(b, carry):
        for core in range(2):
            for col in range(cols):
                for plane in range(planes):
                    r = pl.multiple_of((plane * side + b) * 32 + core * 16, 16)
                    wo[col, pl.ds(r, 16), :] = py[core, b, col, plane]
        return carry

    lax.fori_loop(0, side, place_out, 0)
    for k in range(1, cols):
        from_x = lax.rem(x + cols - k, cols)
        arrive(act.at[from_x, :, pl.ds(0, LANES)], acs.at[k], acr.at[k])
        arrive(act.at[from_x, :, pl.ds(LANES, LANES)], ass.at[k], asr.at[k])

    def out_rows(i, carry):
        r = pl.ds(pl.multiple_of(i * block_rows, block_rows), block_rows)
        total = nt(act[0, r, :], wo[0])
        for col in range(1, cols):
            total = total + nt(act[col, r, :], wo[col])
        out_ref[r, :] = total.astype(BF16)
        return carry

    lax.fori_loop(0, rows // block_rows, out_rows, 0)
    for one in sent:
        one.wait_send()


def on_device(
    side,
    cols,
    tokens,
    norm_gain,
    w_value,
    w_gate,
    w_drive,
    conv_taps,
    conv_gain,
    log_step,
    step_shift,
    state_real,
    state_imag,
    in_map,
    out_map,
    skip_gain,
    start_state,
    conv_proj,
    state_proj,
):
    rows, depth = tokens.shape
    planes = side // cols
    out_cols = planes * side * 32
    groups, states = state_real.shape
    width = groups * states
    hbm = pl.BlockSpec(memory_space=pltpu.HBM)
    vmem = pl.BlockSpec(memory_space=pltpu.VMEM)
    dma = pltpu.SemaphoreType.DMA
    near, line = dma((cols,)), dma((side,))
    return pl.pallas_call(
        functools.partial(kernel, (side, cols)),
        out_shape=jax.ShapeDtypeStruct((rows, out_cols), BF16),
        in_specs=[hbm] * 6 + [vmem] * 11,
        out_specs=vmem,
        scratch_shapes=[
            pltpu.VMEM((rows, depth), BF16),
            pltpu.VMEM((rows, depth), BF16),
            pltpu.VMEM((2, side, side, 16, LANES), BF16),
            pltpu.VMEM((2, side, side, 16, 2 * LANES), BF16),
            pltpu.VMEM((side, 16, 2 * LANES), BF16),
            pltpu.VMEM((2, side, cols, planes, 16, 2 * LANES), BF16),
            pltpu.VMEM((depth, LANES), BF16),
            pltpu.VMEM((depth, 2 * LANES), BF16),
            pltpu.VMEM((cols, out_cols, 2 * LANES), BF16),
            pltpu.VMEM((4, rows, LANES), F32),
            *[pltpu.VMEM((rows, width), F32)] * 6,
            pltpu.VMEM((2, 2, LANES, width), BF16),
            pltpu.VMEM((2, 2, LANES, width), BF16),
            pltpu.VMEM((rows, LANES), F32),
            pltpu.VMEM((rows, LANES), F32),
            pltpu.VMEM((rows + 32, LANES), F32),
            pltpu.VMEM((rows, LANES), F32),
            pltpu.VMEM((32, LANES), BF16),
            pltpu.VMEM((32, LANES), BF16),
            pltpu.VMEM((8, rows), F32),
            pltpu.VMEM((cols - 1, 8, rows), F32),
            pltpu.VMEM((16, LANES), F32),
            pltpu.VMEM((16, LANES), F32),
            pltpu.VMEM((side * 16, LANES), F32),
            pltpu.VMEM((side * 16, LANES), F32),
            pltpu.VMEM((cols, rows, 2 * LANES), BF16),
            dma((6,)),
            *[line] * 10,
            near,
            near,
            line,
            line,
            *[line] * 6,
            dma((2,)),
            dma((2,)),
            *[line] * 4,
            *[near] * 6,
        ],
        compiler_params=pltpu.CompilerParams(
            collective_id=0, has_side_effects=True, vmem_limit_bytes=60 * 1024 * 1024
        ),
    )(
        tokens,
        w_value,
        w_gate,
        w_drive,
        conv_proj.T,
        state_proj.T,
        norm_gain.reshape(1, depth),
        conv_taps,
        conv_gain.reshape(1, -1),
        log_step.reshape(1, -1),
        step_shift.T,
        state_real,
        state_imag,
        jnp.transpose(in_map, (0, 1, 3, 2)).reshape(-1, states),
        out_map.reshape(-1, states),
        skip_gain,
        start_state.reshape(-1, states),
    )


def solution(mesh):
    side = math.isqrt(mesh.shape["sp"] // 2)
    placed = (
        P("sp", None),
        P(),
        P("sp", "tp"),
        P("sp", "tp"),
        P("sp", "tp"),
        P(None, "tp"),
        P("tp"),
        P("tp"),
        P("sp", "tp"),
        P("tp", None),
        P("tp", None),
        P(None, "tp", None, None),
        P(None, "tp", None, None),
        P("tp", None),
        P(None, "tp", None),
        P("tp", "sp"),
        P("tp", "sp"),
    )
    return jax.shard_map(
        functools.partial(on_device, side, mesh.shape["tp"]),
        mesh=mesh,
        in_specs=placed,
        out_specs=P("sp", "tp"),
        check_vma=False,
    )
```

time: 254 us -> 61.2 us (0.24)
  waiting for transfers between devices: 83.2 us -> 0 us
  blocking collectives: 68.6 us -> 0 us
  Pallas kernels: 0 us -> 59.2 us
  other arithmetic: 25.4 us -> 0 us
  local copies, waits for them, and re-layouts: 24 us -> 1.87 us
  starting transfers between devices: 18.1 us -> 0 us
  matrix products: 14.9 us -> 0 us
  between operations: 14.1 us -> 0.01 us
  loops' own time: 5.06 us -> 0 us
    all_gather x2 -> x0, waiting for transfers between devices: 80.8 us -> none  [the longest x1 80.8 us: sent_together(): out = lax.all_gather(both, axis, axis=dim, tiled=True)]
    pallas_call x0 -> x1, Pallas kernels: none -> 59.2 us  [on_device(): pl.pallas_call(functools.partial(kernel, (side, cols)), out_shape=jax.Sha...]
    all_gather x3 -> x0, blocking collectives: 40 us -> none  [gathered_once(): both, at, found = (lax.all_gather(jnp.concatenate(lines), axis), 0, {})]
    all_to_all x1 -> x0, blocking collectives: 28.6 us -> none  [sent_and_summed(): lax.all_to_all(pieces, axis, split_axis=0, concat_axis=0, tiled=True)]
    dot_general x12 -> x0, matrix products: 14.9 us -> none  [the longest x4 5.82 us: sweep(): mapped_re = jnp.dot(drive_block, in_real, precision=lax.Precision.HIGHEST)]
    ppermute x1 -> x0, starting transfers between devices: 14.1 us -> none  [from_behind(): return lax.ppermute(x, axis, pairs)]
    slice x387 -> x0, local copies, waits for them, and re-layouts: 11.8 us -> none  [the longest x364 11.6 us: sweep(): lax.associative_scan(pair_combine, (keep_re, keep_im, input_re, input_im)...]
    dynamic_update_slice x8 -> x0, other arithmetic: 7.57 us -> none  [on_device(): lax.scan(sweep, (zero_row, zero_row, one_row, zero_row), (steps_all, driv...]
  transfers between devices with their start and end apart: 4 -> 0, of which waited for: 2 -> 0; matrix products, arithmetic and copies ran while one was open for 23% -> 0% of each run, Pallas kernels for 0% -> 0%
where the time goes in v1:
time: 61.2 us; the launch traced here: 61 us
  Pallas kernels  59.2 us (97%)
  local copies, waits for them, and re-layouts  1.87 us (3%)
    pallas_call x1, Pallas kernels, on_device(): pl.pallas_call(functools.partial(kernel, (side, cols)), out_shape=jax.Sha...  59.2 us
    unnamed x1, local copies, waits for them, and re-layouts  1.87 us

profile of v1, /device:TPU:1, one launch (start us, length us, event | category | flops | bytes accessed | tf_op | source)
XLA Modules:
  0.0 61.0 jit_solution(15869680410188527564)
XLA Ops:
  0.0 59.2 %shard_map.163 = bf16[512,512]{1,0:T(8,128)(2,1)} custom-call(bf16[512,2048]{1,0:T(8,128)(2,1)} %tokens_hbm.1, bf16[16,128]{1,0:T(8,128)(2,1)} %value_hbm.1, bf16[16,128]{1,0:T(8,128)(2,1)} %gate_hbm.1, bf16[16,128]{1,0:T(8,128)(2,1)} %drive_hbm.1, bf16[16,128]{1,0:T(8,128)(2,1)} %bitcast.16, bf16[16,128]{1,0:T(8,128)(2,1)} %bitcast.17, f32[1,2048]{1,0:T(1,128)} %bitcast.14, ...), custom_call_target="tpu_custom_call" | custom-call | tf_op jit(solution)/shard_map/pallas_call | solution.py:677
  59.2 1.9 %copy.19 = bf16[512,512]{1,0:T(8,128)(2,1)} copy(bf16[512,512]{1,0:T(8,128)(2,1)} %shard_map.163) | data formatting | bytes 1048576

commit v2 on v1

v2 whole, which is shorter than its diff:
```python
import functools
import math

import jax
import jax.numpy as jnp
from jax import lax
from jax.experimental import pallas as pl
from jax.experimental.pallas import tpu as pltpu
from jax.sharding import PartitionSpec as P

MESH = pl.DeviceIdType.MESH
F32, BF16 = jnp.float32, jnp.bfloat16
HIGHEST = lax.Precision.HIGHEST
CHUNKS = 8
LANES = 128
PI_HEAD, PI_MID, PI_TAIL = 3.140625, 9.67502593994140625e-4, 1.509957990978376432e-7
SIN = (
    0.9999999956945582,
    -0.16666657935421791,
    0.008333049779224343,
    -0.00019808982983932522,
    2.605019582042587e-06,
)
COS = (
    0.9999999997785899,
    -0.4999999935376166,
    0.04166663608814349,
    -0.0013888359276841241,
    2.476005397141232e-05,
    -2.6049608226484117e-07,
)


def series(terms, x):
    total = terms[-1]
    for term in reversed(terms[:-1]):
        total = total * x + term
    return total


def keep_of(rate_re, rate_im, step):
    angle = rate_im * step
    turns = jnp.floor(angle * (1.0 / math.pi) + 0.5)
    rest = ((angle - turns * PI_HEAD) - turns * PI_MID) - turns * PI_TAIL
    square = rest * rest
    half = turns * 0.5
    size = jnp.exp(rate_re * step) * (1.0 - 4.0 * (half - jnp.floor(half)))
    return size * series(COS, square), size * (rest * series(SIN, square))


def nn(a, b, precision=None):
    return lax.dot_general(
        a, b, (((1,), (0,)), ((), ())), precision=precision, preferred_element_type=F32
    )


def nt(a, b, precision=None):
    return lax.dot_general(
        a, b, (((1,), (1,)), ((), ())), precision=precision, preferred_element_type=F32
    )


def tn(a, b, precision=None):
    return lax.dot_general(
        a, b, (((0,), (0,)), ((), ())), precision=precision, preferred_element_type=F32
    )


def ids(shape, dim):
    return lax.broadcasted_iota(jnp.int32, shape, dim)


def far_first(side):
    return sorted(range(1, side), key=lambda k: -min(k, side - k))


def split_two(x):
    head = x.astype(BF16)
    return head, (x - head.astype(F32)).astype(BF16)


def entry_of(arrived, side, place, rate_re, rate_im, q):
    real = arrived[pl.ds(q, side, stride=16), :]
    imag = arrived[pl.ds(4 + q, side, stride=16), :]
    step = arrived[pl.ds(8 + q, side, stride=16), :]
    row = ids((side, LANES), 0)
    since = jnp.zeros((side, LANES), F32)
    for k in range(side):
        since = since + jnp.where((row < k) & (place > k), step[k : k + 1], 0.0)
    turn_re, turn_im = keep_of(rate_re, rate_im, since)
    before = row < place
    got_re = jnp.where(before, turn_re * real - turn_im * imag, 0.0)
    got_im = jnp.where(before, turn_re * imag + turn_im * real, 0.0)
    ahead = jnp.where(before, step, 0.0)
    return (
        jnp.sum(got_re, axis=0, keepdims=True),
        jnp.sum(got_im, axis=0, keepdims=True),
        jnp.sum(ahead, axis=0, keepdims=True),
    )


def kernel(
    dims,
    tokens_hbm,
    value_hbm,
    gate_hbm,
    drive_hbm,
    convp_hbm,
    statep_hbm,
    gain_hbm,
    taps_hbm,
    conv_gain_hbm,
    log_step_hbm,
    shift_hbm,
    rate_re_hbm,
    rate_im_hbm,
    in_hbm,
    out_map_hbm,
    skip_hbm,
    start_hbm,
    out_ref,
    gain_ref,
    taps_ref,
    conv_gain_ref,
    log_step_ref,
    shift_ref,
    rate_re_ref,
    rate_im_ref,
    in_ref,
    out_map_ref,
    skip_ref,
    start_ref,
    tok,
    nrm,
    gd,
    gv,
    pz,
    py,
    wd,
    wvg,
    wo_conv,
    wo_state,
    dtx,
    kr,
    ki,
    cr,
    ci,
    mm,
    in_blocks,
    out_blocks,
    drv,
    drvp,
    gf,
    cm,
    halo,
    halo_send,
    st_all,
    st_rows,
    mc_send,
    mc_recv,
    my_all,
    mz_all,
    mix_all,
    conv_all,
    state_all,
    acc,
    sems,
):
    side, cols = dims
    rows, depth = tokens_hbm.shape
    planes = side // cols
    sp, x = lax.axis_index("sp"), lax.axis_index("tp")
    c = lax.rem(sp, 2)
    chip = lax.div(sp, 2)
    y, z = lax.rem(chip, side), lax.div(chip, side)
    count = 2 * side * side
    steps = rows // CHUNKS
    wide = 4 * LANES
    free = iter(range(sems.shape[0]))

    def new_sems(n):
        return [sems.at[next(free)] for _ in range(n)]

    def at(zz, yy, cc):
        return (zz * side + yy) * 2 + cc

    def turn(a, k):
        return lax.rem(a + k, side)

    mate = at(z, y, 1 - c)
    b_me, a_me = c * z + (1 - c) * y, c * y + (1 - c) * z

    def b_peer(b):
        return c * at(b, y, 1) + (1 - c) * at(z, b, 0)

    def a_peer(a):
        return c * at(z, a, 1) + (1 - c) * at(a, y, 0)

    beyond = lax.rem(sp + 2 * c - 1 + count, count)
    following = lax.rem(sp + 1, count)

    def copy(src, dst, send_sem, recv_sem, to_sp, to_x):
        return pltpu.make_async_remote_copy(
            src_ref=src,
            dst_ref=dst,
            send_sem=send_sem,
            recv_sem=recv_sem,
            device_id=(to_sp, to_x),
            device_id_type=MESH,
        )

    outgoing = []

    def group(total):
        (sem,) = new_sems(1)
        outgoing.append((total, sem))
        return sem

    def send(src, dst, send_sem, recv_sem, to_sp, to_x):
        copy(src, dst, send_sem, recv_sem, to_sp, to_x).start()

    def arrive(dst, recv_sem):
        copy(dst, dst, recv_sem, recv_sem, mate, x).wait_recv()

    barrier = pltpu.get_barrier_semaphore()

    def greet(to_sp, to_x):
        pl.semaphore_signal(barrier, inc=1, device_id=(to_sp, to_x), device_id_type=MESH)

    for k in far_first(side):
        greet(at(z, turn(y, k), c), x)
        greet(at(turn(z, k), y, c), x)
    for k in far_first(cols):
        greet(sp, lax.rem(x + k, cols))
    greet(beyond, x)
    greet(mate, x)

    pairs = [
        (drive_hbm, gd.at[c, a_me, b_me]),
        (value_hbm, gv.at[c, a_me, b_me, :, pl.ds(0, LANES)]),
        (gate_hbm, gv.at[c, a_me, b_me, :, pl.ds(LANES, LANES)]),
        (convp_hbm, pz.at[z, :, pl.ds(0, LANES)]),
        (statep_hbm, pz.at[z, :, pl.ds(LANES, LANES)]),
        (in_hbm, in_ref),
        (out_map_hbm, out_map_ref),
        (rate_re_hbm, rate_re_ref),
        (rate_im_hbm, rate_im_ref),
        (start_hbm, start_ref),
        (skip_hbm, skip_ref),
        (log_step_hbm, log_step_ref),
        (shift_hbm, shift_ref),
        (gain_hbm, gain_ref),
        (taps_hbm, taps_ref),
        (conv_gain_hbm, conv_gain_ref),
        (tokens_hbm, tok),
    ]
    own_copies = [
        pltpu.make_async_copy(src, dst, sem) for (src, dst), sem in zip(pairs, new_sems(len(pairs)))
    ]
    for one in own_copies:
        one.start()
    for one in own_copies[:5]:
        one.wait()

    pl.semaphore_wait(barrier, 2 * side + cols - 1)
    d1_all, v1_all, p1_all, p2_all = new_sems(4)
    here = gd.at[c, a_me, b_me]
    sem = group(gd.at[c, a_me, pl.ds(0, side - 1)])
    for k in far_first(side):
        send(here, here, sem, d1_all, b_peer(turn(b_me, k)), x)
    here = gv.at[c, a_me, b_me]
    sem = group(gv.at[c, a_me, pl.ds(0, side - 1)])
    for k in far_first(side):
        send(here, here, sem, v1_all, b_peer(turn(b_me, k)), x)
    here = pz.at[z]
    sem = group(pz.at[pl.ds(0, side - 1)])
    for k in far_first(side):
        send(here, here, sem, p1_all, at(turn(z, k), y, c), x)

    for one in own_copies[5:13]:
        one.wait()
    group_mask = (ids((LANES, wide), 1) // 64 == ids((LANES, wide), 0) // 16).astype(F32)
    spread = (ids((64, wide), 1) % 64 == ids((64, wide), 0)).astype(F32)
    for part in range(2):
        rows_here, cols_here = pl.ds(part * LANES, LANES), pl.ds(part * wide, wide)
        first, rest = split_two(nn(in_ref[rows_here, :], spread, HIGHEST) * group_mask)
        in_blocks[part, pl.ds(0, LANES), :] = first
        in_blocks[part, pl.ds(LANES, LANES), :] = rest
        sign = 1.0 - 2.0 * part
        first, rest = split_two(nn(out_map_ref[rows_here, :], spread, HIGHEST) * (sign * group_mask))
        out_blocks[pl.ds(0, LANES), cols_here] = first
        out_blocks[pl.ds(LANES, LANES), cols_here] = rest
    own_group = (ids((8, wide), 1) // 64 == ids((8, wide), 0)).astype(F32)

    def flat(value):
        return jnp.sum(nn(value, spread, HIGHEST) * own_group, axis=0, keepdims=True)

    rate_re, rate_im = flat(rate_re_ref[...]), flat(rate_im_ref[...])
    first_re, first_im = flat(start_ref[0:8, :]), flat(start_ref[8:16, :])
    size = rate_re * rate_re + rate_im * rate_im
    inv_re, inv_im = rate_re / size, rate_im / size
    spread16 = (ids((16, LANES), 1) % 16 == ids((16, LANES), 0)).astype(F32)
    own16 = (ids((8, LANES), 1) // 16 == ids((8, LANES), 0)).astype(F32)
    skip_row = jnp.sum(nn(skip_ref[...], spread16, HIGHEST) * own16, axis=0, keepdims=True)
    eye8 = ids((8, 8), 0) == ids((8, 8), 1)
    log_step = jnp.sum(jnp.where(eye8, log_step_ref[...], 0.0), axis=1, keepdims=True)
    dt = jnp.exp(log_step + shift_ref[...])

    def tile(v, q):
        return v[:, q * LANES : (q + 1) * LANES]

    for q in range(4):
        dtx[q] = tn(dt, tile(own_group, q), HIGHEST)

    for one in own_copies[13:]:
        one.wait()
    gain = gain_ref[...]

    def norm_rows(i, carry):
        r = pl.ds(pl.multiple_of(i * 16, 16), 16)
        wide_rows = tok[r, :].astype(F32)
        mean = jnp.sum(wide_rows * wide_rows, axis=1, keepdims=True) * (1.0 / depth)
        nrm[r, :] = (wide_rows * lax.rsqrt(mean + 1e-06) * gain).astype(BF16)
        return carry

    lax.fori_loop(0, rows // 16, norm_rows, 0, unroll=4)

    d2_from, v2_from = new_sems(side - 1), new_sems(side - 1)
    dc_all, vc_all, pc_all = new_sems(3)
    arrive(gd.at[c, a_me, pl.ds(0, side - 1)], d1_all)
    line = gd.at[c, a_me]
    sem, dc_sem = group(gd.at[c, pl.ds(0, side - 1)]), group(gd.at[c])
    for k in far_first(side):
        send(line, line, sem, d2_from[k - 1], a_peer(turn(a_me, k)), x)
    send(line, line, dc_sem, dc_all, mate, x)

    arrive(gv.at[c, a_me, pl.ds(0, side - 1)], v1_all)
    line = gv.at[c, a_me]
    sem, vc_sem = group(gv.at[c, pl.ds(0, side - 1)]), group(gv.at[c])
    for k in far_first(side):
        send(line, line, sem, v2_from[k - 1], a_peer(turn(a_me, k)), x)
    send(line, line, vc_sem, vc_all, mate, x)
    arrive(pz.at[pl.ds(0, side - 1)], p1_all)
    sem = group(pz.at[pl.ds(0, (cols - 1) * planes)])
    for k in far_first(cols):
        to = lax.rem(x + k, cols)
        send(pz.at[pl.ds(to * planes, planes)], py.at[c, y, x], sem, p2_all, sp, to)
    py[c, y, x] = pz[pl.ds(x * planes, planes)]

    def keep_rows(j, carry):
        r = pl.ds(pl.multiple_of(j * 8, 8), 8)
        new = []
        for q in range(4):
            step = dtx[q, pl.ds(j, CHUNKS, stride=steps), :]
            keep_re, keep_im = keep_of(tile(rate_re, q), tile(rate_im, q), step)
            minus = keep_re - 1.0
            cols_q = pl.ds(q * LANES, LANES)
            kr[r, cols_q] = keep_re
            ki[r, cols_q] = keep_im
            cr[r, cols_q] = minus * tile(inv_re, q) + keep_im * tile(inv_im, q)
            ci[r, cols_q] = keep_im * tile(inv_re, q) - minus * tile(inv_im, q)
            new.append(carry[q] + step)
        return tuple(new)

    zero = jnp.zeros((CHUNKS, LANES), F32)
    spans = lax.fori_loop(0, steps, keep_rows, (zero,) * 4, unroll=2)

    for k in reversed(far_first(side)):
        block = gd.at[c, turn(a_me, side - k)]
        arrive(block, d2_from[k - 1])
        send(block, block, dc_sem, dc_all, mate, x)

    arrive(gd.at[1 - c], dc_all)

    def place_drive(a, carry):
        for b in range(side):
            r = pl.multiple_of(at(a, b, 0) * 16, 16)
            wd[pl.ds(r, 16), :] = gd[0, a, b]
            r = pl.multiple_of(at(b, a, 1) * 16, 16)
            wd[pl.ds(r, 16), :] = gd[1, a, b]
        return carry

    lax.fori_loop(0, side, place_drive, 0)
    block_rows = min(rows, 256)

    def blocks(body):
        for i in range(rows // block_rows):
            body(pl.ds(i * block_rows, block_rows))

    def drive_rows(r):
        drv[r, :] = nn(nrm[r, :], wd[...]).astype(BF16).astype(F32)

    blocks(drive_rows)

    def turn_rows(j, carry):
        r = pl.ds(pl.multiple_of(j * 8, 8), 8)
        drvp[r, :] = drv[pl.ds(j, CHUNKS, stride=steps), :]
        return carry

    lax.fori_loop(0, steps, turn_rows, 0, unroll=8)

    def map_rows(r):
        d = drvp[r, :].astype(BF16)
        d = jnp.concatenate([d, d], axis=1)
        mm[r, pl.ds(0, wide)] = nn(d, in_blocks[0])
        mm[r, pl.ds(wide, wide)] = nn(d, in_blocks[1])

    blocks(map_rows)

    def scan_rows(j, carry):
        r = pl.ds(pl.multiple_of(j * 8, 8), 8)
        new = []
        for q in range(4):
            cols_q = pl.ds(q * LANES, LANES)
            s_re, s_im = carry[2 * q], carry[2 * q + 1]
            c_re, c_im = cr[r, cols_q], ci[r, cols_q]
            m_re, m_im = mm[r, cols_q], mm[r, pl.ds(wide + q * LANES, LANES)]
            u_re = c_re * m_re - c_im * m_im
            u_im = c_re * m_im + c_im * m_re
            cr[r, cols_q] = u_re
            ci[r, cols_q] = u_im
            k_re, k_im = kr[r, cols_q], ki[r, cols_q]
            new.append((k_re * s_re + u_re) - k_im * s_im)
            new.append((k_re * s_im + u_im) + k_im * s_re)
        return tuple(new)

    finals = lax.fori_loop(0, steps, scan_rows, (zero,) * 8, unroll=2)

    row8 = ids((CHUNKS, LANES), 0)
    starts, mine, ahead_spans = [], [], []
    for q in range(4):
        re_q, im_q = tile(rate_re, q), tile(rate_im, q)
        hop_re, hop_im = keep_of(re_q, im_q, spans[q])
        f_re, f_im = finals[2 * q], finals[2 * q + 1]
        e_re = e_im = total = jnp.zeros((1, LANES), F32)
        l_re = l_im = ahead = zero
        for s in range(CHUNKS):
            l_re = jnp.where(row8 == s, e_re, l_re)
            l_im = jnp.where(row8 == s, e_im, l_im)
            ahead = jnp.where(row8 == s, total, ahead)
            h_re, h_im = hop_re[s : s + 1], hop_im[s : s + 1]
            e_re, e_im = (
                h_re * e_re - h_im * e_im + f_re[s : s + 1],
                h_re * e_im + h_im * e_re + f_im[s : s + 1],
            )
            total = total + spans[q][s : s + 1]
        starts.append((l_re, l_im))
        ahead_spans.append(ahead)
        mine.append((e_re, e_im, total))
        mc_send[q : q + 1, :] = e_re
        mc_send[4 + q : 5 + q, :] = e_im
        mc_send[8 + q : 9 + q, :] = total
    mc_send[12:16, :] = jnp.zeros((4, LANES), F32)
    mc_in, halo_in, cy_all, cz_all = new_sems(4)
    send(mc_send, mc_recv, group(mc_send), mc_in, mate, x)

    arrive(mc_recv, mc_in)
    core_entry = []
    second = c == 1
    slot = pl.multiple_of(y * 16, 16)
    for q in range(4):
        re_q, im_q = tile(rate_re, q), tile(rate_im, q)
        m_re, m_im, m_span = mine[q]
        o_re, o_im = mc_recv[q : q + 1, :], mc_recv[4 + q : 5 + q, :]
        o_span = mc_recv[8 + q : 9 + q, :]
        a_re, a_im = jnp.where(second, o_re, m_re), jnp.where(second, o_im, m_im)
        b_re, b_im = jnp.where(second, m_re, o_re), jnp.where(second, m_im, o_im)
        h_re, h_im = keep_of(re_q, im_q, jnp.where(second, m_span, o_span))
        my_all[pl.ds(slot + q, 1), :] = h_re * a_re - h_im * a_im + b_re
        my_all[pl.ds(slot + 4 + q, 1), :] = h_re * a_im + h_im * a_re + b_im
        my_all[pl.ds(slot + 8 + q, 1), :] = m_span + o_span
        none = jnp.zeros_like(o_re)
        core_entry.append(
            (
                jnp.where(second, o_re, none),
                jnp.where(second, o_im, none),
                jnp.where(second, o_span, none),
            )
        )
    part_rows = (side - 1) * 12
    here = my_all.at[pl.ds(slot, 12), :]
    sem = group(my_all.at[pl.ds(0, part_rows), :])
    for k in far_first(side):
        send(here, here, sem, cy_all, at(z, turn(y, k), c), x)

    arrive(pz.at[pl.ds(0, (cols - 1) * planes)], p2_all)
    p3_from = new_sems(side)
    p3_sem, pc_sem = group(py.at[c, pl.ds(0, side - 1)]), group(py.at[c])
    heading = 1 - 2 * c
    ahead_steps, back_steps = side // 2, (side - 1) // 2

    def along(k):
        return lax.rem(y + k * heading + side, side)

    def ring(step):
        if step > 1:
            for k, order, steps_there in (
                (-(step - 1), step - 1, ahead_steps),
                (step - 1, ahead_steps + step - 1, back_steps),
            ):
                if step - 1 <= steps_there:
                    block = py.at[c, along(k)]
                    arrive(block, p3_from[order])
                    send(block, block, pc_sem, pc_all, mate, x)
        for k, order, steps_there, to in (
            (-(step - 1), step, ahead_steps, 1),
            (step - 1, ahead_steps + step, back_steps, -1),
        ):
            if step <= steps_there:
                block = py.at[c, along(k)]
                send(block, block, p3_sem, p3_from[order], at(z, along(to), c), x)

    ring(1)
    line = py.at[c, y]
    send(line, line, pc_sem, pc_all, mate, x)

    for k in reversed(far_first(side)):
        block = gv.at[c, turn(a_me, side - k)]
        arrive(block, v2_from[k - 1])
        send(block, block, vc_sem, vc_all, mate, x)

    arrive(gv.at[1 - c], vc_all)

    def place_value(a, carry):
        for b in range(side):
            r = pl.multiple_of(at(a, b, 0) * 16, 16)
            wvg[pl.ds(r, 16), :] = gv[0, a, b]
            r = pl.multiple_of(at(b, a, 1) * 16, 16)
            wvg[pl.ds(r, 16), :] = gv[1, a, b]
        return carry

    lax.fori_loop(0, side, place_value, 0)

    def gate_rows(r):
        both = nn(nrm[r, :], wvg[...]).astype(BF16).astype(F32)
        gated = (both[:, :LANES] * jax.nn.sigmoid(both[:, LANES:])).astype(BF16)
        gf[pl.ds(r.start + 32, block_rows), :] = gated.astype(F32)

    blocks(gate_rows)
    halo_send[...] = gf[rows : rows + 32, :].astype(BF16)
    send(halo_send, halo, group(halo_send), halo_in, following, x)

    arrive(my_all.at[pl.ds(0, part_rows), :], cy_all)
    chip_entry = []
    slot_z = pl.multiple_of(z * 16, 16)
    for q in range(4):
        re_q, im_q = tile(rate_re, q), tile(rate_im, q)
        chip_entry.append(entry_of(my_all, side, y, re_q, im_q, q))
        all_re, all_im, all_span = entry_of(my_all, side, side, re_q, im_q, q)
        mz_all[pl.ds(slot_z + q, 1), :] = all_re
        mz_all[pl.ds(slot_z + 4 + q, 1), :] = all_im
        mz_all[pl.ds(slot_z + 8 + q, 1), :] = all_span
    here = mz_all.at[pl.ds(slot_z, 12), :]
    sem = group(mz_all.at[pl.ds(0, part_rows), :])
    for k in far_first(side):
        send(here, here, sem, cz_all, at(turn(z, k), y, c), x)

    ring(2)

    arrive(halo, halo_in)

    gf[0:32, :] = jnp.where(sp == 0, 0.0, halo[...].astype(F32))
    taps = taps_ref.shape[0]
    conv_rows = min(rows, 64)

    def conv_block(i, carry):
        base = pl.multiple_of(i * conv_rows, conv_rows)
        total = jnp.zeros((conv_rows, LANES), F32)
        for k in range(taps):
            total = total + taps_ref[k : k + 1, :] * gf[pl.ds(base + (33 - taps) + k, conv_rows), :]
        cm[pl.ds(base, conv_rows), :] = total
        return carry

    lax.fori_loop(0, rows // conv_rows, conv_block, 0)

    mix = cm[...]
    own_mean = nn(mix, jnp.full((LANES, LANES), 1.0 / LANES, F32), HIGHEST)
    lane_x = pl.multiple_of(x * LANES, LANES)
    mix_all[:, pl.ds(lane_x, LANES)] = (mix - own_mean).astype(BF16)
    ones = jnp.ones((8, LANES), F32)
    row_st = ids((8, rows), 0)
    sums = nt(ones, mix, HIGHEST)
    squares = nt(ones, mix * mix, HIGHEST)
    st_all[x] = jnp.where(row_st == 0, sums, jnp.where(row_st == 1, squares, 0.0))
    st_all[x, 2:3, 0:LANES] = conv_gain_ref[...]
    (st_in,) = new_sems(1)
    here = st_all.at[x]
    sem = group(st_all.at[pl.ds(0, cols - 1)])
    for k in far_first(cols):
        send(here, here, sem, st_in, sp, lax.rem(x + k, cols))
    half = rows // 2
    right, left = lax.rem(x + 1, cols), lax.rem(x + cols - 1, cols)
    across = lax.rem(x + 2, cols)

    class Spread:
        def __init__(self, buffer):
            self.buffer = buffer
            self.sem = group(buffer.at[:, pl.ds(0, (cols - 1) * LANES)])
            self.arrivals = new_sems(6 if cols > 2 else 2)

        def part(self, col, first):
            lanes = pl.ds(pl.multiple_of(col * LANES, LANES), LANES)
            return self.buffer.at[pl.ds(0 if first else half, half), lanes]

        def push(self, col, first, order, to):
            block = self.part(col, first)
            send(block, block, self.sem, self.arrivals[order], sp, to)

        def pull(self, col, first, order):
            arrive(self.part(col, first), self.arrivals[order])

        def begin(self):
            self.push(x, 1, 0, right)
            if cols > 2:
                self.push(x, 0, 2, left)
            self.push(x, 0, 1, right)
            if cols > 2:
                self.push(x, 1, 3, left)

        def pass_on(self):
            if cols > 2:
                self.pull(left, 1, 0)
                self.push(left, 1, 4, right)
                self.pull(right, 0, 2)
                self.push(right, 0, 5, left)

        def finish(self):
            if cols == 2:
                self.pull(left, 1, 0)
            self.pull(left, 0, 1)
            if cols > 2:
                self.pull(right, 1, 3)
                self.pull(across, 1, 4)
                self.pull(across, 0, 5)

    mix_spread = Spread(mix_all)
    mix_spread.begin()

    ring(3)

    arrive(mz_all.at[pl.ds(0, part_rows), :], cz_all)

    begin = []
    for q in range(4):
        re_q, im_q = tile(rate_re, q), tile(rate_im, q)
        s_re, s_im = tile(first_re, q), tile(first_im, q)
        for more_re, more_im, span in (
            entry_of(mz_all, side, z, re_q, im_q, q),
            chip_entry[q],
            core_entry[q],
        ):
            h_re, h_im = keep_of(re_q, im_q, span)
            s_re, s_im = h_re * s_re - h_im * s_im + more_re, h_re * s_im + h_im * s_re + more_im
        h_re, h_im = keep_of(re_q, im_q, ahead_spans[q])
        begin.append(h_re * s_re - h_im * s_im + starts[q][0])
        begin.append(h_re * s_im + h_im * s_re + starts[q][1])

    ring(4)

    def state_rows(j, carry):
        r = pl.ds(pl.multiple_of(j * 8, 8), 8)
        new = []
        for q in range(4):
            cols_q = pl.ds(q * LANES, LANES)
            s_re, s_im = carry[2 * q], carry[2 * q + 1]
            k_re, k_im = kr[r, cols_q], ki[r, cols_q]
            n_re = (k_re * s_re + cr[r, cols_q]) - k_im * s_im
            n_im = (k_re * s_im + ci[r, cols_q]) + k_im * s_re
            mm[r, cols_q] = n_re
            mm[r, pl.ds(wide + q * LANES, LANES)] = n_im
            new.extend((n_re, n_im))
        return tuple(new)

    lax.fori_loop(0, steps, state_rows, tuple(begin), unroll=2)

    def read_rows(r):
        first, rest = split_two(mm[r, :])
        total = nt(first, out_blocks[...])
        total = total[:, :LANES] + total[:, LANES:] + nt(rest, out_blocks[pl.ds(0, LANES), :])
        drvp[r, :] = jax.nn.gelu(total + skip_row * drvp[r, :])

    blocks(read_rows)

    def back_rows(j, carry):
        r = pl.ds(pl.multiple_of(j * 8, 8), 8)
        drv[pl.ds(j, CHUNKS, stride=steps), :] = drvp[r, :]
        return carry

    lax.fori_loop(0, steps, back_rows, 0, unroll=8)
    state_all[:, pl.ds(lane_x, LANES)] = drv[...].astype(BF16)

    mix_spread.pass_on()
    state_spread = Spread(state_all)
    state_spread.begin()

    for step in range(5, ahead_steps + 2):
        ring(step)

    arrive(st_all.at[pl.ds(0, cols - 1)], st_in)
    channels = cols * LANES
    mean = sum(st_all[k, 0:1, :] for k in range(cols)) * (1.0 / channels)
    square = sum(st_all[k, 1:2, :] for k in range(cols)) * (1.0 / channels)
    inv = lax.rsqrt(square - mean * mean + 1e-05)
    table = jnp.where(row_st == 0, inv, 0.0)
    for k in range(cols):
        offset = (st_all[k, 0:1, :] * (1.0 / LANES) - mean) * inv
        table = jnp.where(row_st == 1 + k, offset, table)
    st_rows[...] = table
    pick = ids((8, LANES), 0)

    def apply_norm(col):
        lanes = pl.ds(pl.multiple_of(col * LANES, LANES), LANES)
        scale = tn(st_rows[...], (pick == 0).astype(F32), HIGHEST)
        offset = tn(st_rows[...], (pick == 1 + col).astype(F32), HIGHEST)
        value = mix_all[:, lanes].astype(F32) * scale + offset
        value = value * st_all[col, 2:3, 0:LANES]
        conv_all[:, lanes] = (value * jax.nn.sigmoid(value)).astype(BF16)

    apply_norm(x)

    state_spread.pass_on()

    mix_spread.finish()

    for k in range(1, cols):
        apply_norm(lax.rem(x + k, cols))

    arrive(py.at[1 - c], pc_all)

    def place_out(b, carry):
        for core in range(2):
            for col in range(cols):
                for plane in range(planes):
                    r = pl.ds(pl.multiple_of((plane * side + b) * 32 + core * 16, 16), 16)
                    piece = py[core, b, col, plane]
                    wo_conv[r, pl.ds(col * LANES, LANES)] = piece[:, :LANES]
                    wo_state[r, pl.ds(col * LANES, LANES)] = piece[:, LANES:]
        return carry

    lax.fori_loop(0, side, place_out, 0)

    def early_rows(r):
        acc[r, :] = nt(conv_all[r, :], wo_conv[...])

    blocks(early_rows)

    state_spread.finish()

    def late_rows(r):
        out_ref[r, :] = (acc[r, :] + nt(state_all[r, :], wo_state[...])).astype(BF16)

    blocks(late_rows)

    for total, sem in outgoing:
        copy(total, total, sem, sem, mate, x).wait_send()
    assert next(free, None) is None


def sem_count(side, cols):
    operands, groups = 17, 17
    return operands + groups + 2 * (side - 1) + side + 3 + 4 + 4 + 1 + 2 * (6 if cols > 2 else 2)


def on_device(
    side,
    cols,
    tokens,
    norm_gain,
    w_value,
    w_gate,
    w_drive,
    conv_taps,
    conv_gain,
    log_step,
    step_shift,
    state_real,
    state_imag,
    in_map,
    out_map,
    skip_gain,
    start_state,
    conv_proj,
    state_proj,
):
    rows, depth = tokens.shape
    planes = side // cols
    out_cols = planes * side * 32
    groups, states = state_real.shape
    width = groups * states
    hbm = pl.BlockSpec(memory_space=pl.ANY)
    vmem = pl.BlockSpec(memory_space=pltpu.VMEM)
    small = (
        norm_gain.reshape(1, depth),
        conv_taps,
        conv_gain.reshape(1, -1),
        log_step.reshape(1, -1),
        step_shift.T,
        state_real,
        state_imag,
        jnp.transpose(in_map, (0, 1, 3, 2)).reshape(-1, states),
        out_map.reshape(-1, states),
        skip_gain,
        start_state.reshape(-1, states),
    )
    return pl.pallas_call(
        functools.partial(kernel, (side, cols)),
        out_shape=pltpu.VMEM((rows, out_cols), BF16),
        in_specs=[hbm] * 17,
        out_specs=vmem,
        scratch_shapes=[
            *[pltpu.VMEM(a.shape, F32) for a in small],
            pltpu.VMEM((rows, depth), BF16),
            pltpu.VMEM((rows, depth), BF16),
            pltpu.VMEM((2, side, side, 16, LANES), BF16),
            pltpu.VMEM((2, side, side, 16, 2 * LANES), BF16),
            pltpu.VMEM((side, 16, 2 * LANES), BF16),
            pltpu.VMEM((2, side, cols, planes, 16, 2 * LANES), BF16),
            pltpu.VMEM((depth, LANES), BF16),
            pltpu.VMEM((depth, 2 * LANES), BF16),
            pltpu.VMEM((out_cols, cols * LANES), BF16),
            pltpu.VMEM((out_cols, cols * LANES), BF16),
            pltpu.VMEM((4, rows, LANES), F32),
            *[pltpu.VMEM((rows, width), F32)] * 4,
            pltpu.VMEM((rows, 2 * width), F32),
            pltpu.VMEM((2, 2 * LANES, width), BF16),
            pltpu.VMEM((2 * LANES, 2 * width), BF16),
            pltpu.VMEM((rows, LANES), F32),
            pltpu.VMEM((rows, LANES), F32),
            pltpu.VMEM((rows + 32, LANES), F32),
            pltpu.VMEM((rows, LANES), F32),
            pltpu.VMEM((32, LANES), BF16),
            pltpu.VMEM((32, LANES), BF16),
            pltpu.VMEM((cols, 8, rows), F32),
            pltpu.VMEM((8, rows), F32),
            pltpu.VMEM((16, LANES), F32),
            pltpu.VMEM((16, LANES), F32),
            pltpu.VMEM((side * 16, LANES), F32),
            pltpu.VMEM((side * 16, LANES), F32),
            *[pltpu.VMEM((rows, cols * LANES), BF16)] * 3,
            pltpu.VMEM((rows, out_cols), F32),
            pltpu.SemaphoreType.DMA((sem_count(side, cols),)),
        ],
        compiler_params=pltpu.CompilerParams(
            collective_id=0, has_side_effects=True, vmem_limit_bytes=60 * 1024 * 1024
        ),
    )(
        tokens,
        w_value,
        w_gate,
        w_drive,
        conv_proj.T,
        state_proj.T,
        *small,
    )


def solution(mesh):
    side = math.isqrt(mesh.shape["sp"] // 2)
    placed = (
        P("sp", None),
        P(),
        P("sp", "tp"),
        P("sp", "tp"),
        P("sp", "tp"),
        P(None, "tp"),
        P("tp"),
        P("tp"),
        P("sp", "tp"),
        P("tp", None),
        P("tp", None),
        P(None, "tp", None, None),
        P(None, "tp", None, None),
        P("tp", None),
        P(None, "tp", None),
        P("tp", "sp"),
        P("tp", "sp"),
    )
    return jax.shard_map(
        functools.partial(on_device, side, mesh.shape["tp"]),
        mesh=mesh,
        in_specs=placed,
        out_specs=P("sp", "tp"),
        check_vma=False,
    )
```

time: 61.2 us -> 54.9 us (0.90)
  the two profiles are of different devices: /device:TPU:1 before, /device:TPU:2 now
where the time goes in v2:
time: 54.9 us; the launch traced here: 54.8 us
  Pallas kernels  54 us (98%)
  local copies, waits for them, and re-layouts  0.8 us (1%)
    pallas_call x1, Pallas kernels, on_device(): pl.pallas_call(functools.partial(kernel, (side, cols)), out_shape=pltpu.V...  54 us

profile of v2, /device:TPU:2, one launch (start us, length us, event | category | flops | bytes accessed | tf_op | source)
XLA Modules:
  0.0 54.8 jit_solution(11326261816191915788)
XLA Ops:
  0.0 54.0 %shard_map.163 = bf16[512,512]{1,0:T(8,128)(2,1)S(1)} custom-call(bf16[512,2048]{1,0:T(8,128)(2,1)} %tokens_hbm.1, bf16[16,128]{1,0:T(8,128)(2,1)} %value_hbm.1, bf16[16,128]{1,0:T(8,128)(2,1)} %gate_hbm.1, bf16[16,128]{1,0:T(8,128)(2,1)} %drive_hbm.1, bf16[16,128]{1,0:T(8,128)(2,1)} %bitcast.16, bf16[16,128]{1,0:T(8,128)(2,1)} %bitcast.17, ...), custom_call_target="tpu_custom_call" | custom-call | tf_op jit(solution)/shard_map/pallas_call | solution.py:805
  54.0 0.8 %copy.19 = bf16[512,512]{1,0:T(8,128)(2,1)} copy(bf16[512,512]{1,0:T(8,128)(2,1)S(1)} %shard_map.163) | data formatting | bytes 1048576

commit v3 on v2

--- a/solution.py
+++ b/solution.py
@@ -135,7 +135,7 @@
     gd,
     gv,
     pz,
-    py,
+    gp,
     wd,
     wvg,
     wo_conv,
@@ -196,6 +196,13 @@
     def a_peer(a):
         return c * at(z, a, 1) + (1 - c) * at(a, y, 0)
 
+    shift = side // 2
+    piece_z = lax.rem(lax.rem(z, planes) * cols + x + shift, side)
+    piece_x = lax.div(z, planes)
+    piece_a, piece_b = c * y + (1 - c) * piece_z, c * piece_z + (1 - c) * y
+    order = lax.rem(z + side - shift, side)
+    from_z, from_x = x * planes + lax.div(order, cols), lax.rem(order, cols)
+
     beyond = lax.rem(sp + 2 * c - 1 + count, count)
     following = lax.rem(sp + 1, count)
 
@@ -232,6 +239,8 @@
         greet(at(turn(z, k), y, c), x)
     for k in far_first(cols):
         greet(sp, lax.rem(x + k, cols))
+    greet(at(piece_z, y, c), piece_x)
+    greet(at(from_z, y, c), from_x)
     greet(beyond, x)
     greet(mate, x)
 
@@ -239,8 +248,8 @@
         (drive_hbm, gd.at[c, a_me, b_me]),
         (value_hbm, gv.at[c, a_me, b_me, :, pl.ds(0, LANES)]),
         (gate_hbm, gv.at[c, a_me, b_me, :, pl.ds(LANES, LANES)]),
-        (convp_hbm, pz.at[z, :, pl.ds(0, LANES)]),
-        (statep_hbm, pz.at[z, :, pl.ds(LANES, LANES)]),
+        (convp_hbm, pz.at[:, pl.ds(0, LANES)]),
+        (statep_hbm, pz.at[:, pl.ds(LANES, LANES)]),
         (in_hbm, in_ref),
         (out_map_hbm, out_map_ref),
         (rate_re_hbm, rate_re_ref),
@@ -262,8 +271,8 @@
     for one in own_copies[:5]:
         one.wait()
 
-    pl.semaphore_wait(barrier, 2 * side + cols - 1)
-    d1_all, v1_all, p1_all, p2_all = new_sems(4)
+    pl.semaphore_wait(barrier, 2 * side + cols + 1)
+    d1_all, v1_all, p0_in, p1_all = new_sems(4)
     here = gd.at[c, a_me, b_me]
     sem = group(gd.at[c, a_me, pl.ds(0, side - 1)])
     for k in far_first(side):
@@ -272,10 +281,7 @@
     sem = group(gv.at[c, a_me, pl.ds(0, side - 1)])
     for k in far_first(side):
         send(here, here, sem, v1_all, b_peer(turn(b_me, k)), x)
-    here = pz.at[z]
-    sem = group(pz.at[pl.ds(0, side - 1)])
-    for k in far_first(side):
-        send(here, here, sem, p1_all, at(turn(z, k), y, c), x)
+    send(pz, gp.at[c, piece_a, piece_b], group(pz), p0_in, at(piece_z, y, c), piece_x)
 
     for one in own_copies[5:13]:
         one.wait()
@@ -325,7 +331,7 @@
 
     lax.fori_loop(0, rows // 16, norm_rows, 0, unroll=4)
 
-    d2_from, v2_from = new_sems(side - 1), new_sems(side - 1)
+    d2_from, v2_from, p2_from = (new_sems(side - 1) for _ in range(3))
     dc_all, vc_all, pc_all = new_sems(3)
     arrive(gd.at[c, a_me, pl.ds(0, side - 1)], d1_all)
     line = gd.at[c, a_me]
@@ -340,12 +346,11 @@
     for k in far_first(side):
         send(line, line, sem, v2_from[k - 1], a_peer(turn(a_me, k)), x)
     send(line, line, vc_sem, vc_all, mate, x)
-    arrive(pz.at[pl.ds(0, side - 1)], p1_all)
-    sem = group(pz.at[pl.ds(0, (cols - 1) * planes)])
-    for k in far_first(cols):
-        to = lax.rem(x + k, cols)
-        send(pz.at[pl.ds(to * planes, planes)], py.at[c, y, x], sem, p2_all, sp, to)
-    py[c, y, x] = pz[pl.ds(x * planes, planes)]
+    here = gp.at[c, a_me, b_me]
+    arrive(here, p0_in)
+    sem = group(gp.at[c, a_me, pl.ds(0, side - 1)])
+    for k in far_first(side):
+        send(here, here, sem, p1_all, b_peer(turn(b_me, k)), x)
 
     def keep_rows(j, carry):
         r = pl.ds(pl.multiple_of(j * 8, 8), 8)
@@ -451,8 +456,18 @@
         mc_send[4 + q : 5 + q, :] = e_im
         mc_send[8 + q : 9 + q, :] = total
     mc_send[12:16, :] = jnp.zeros((4, LANES), F32)
-    mc_in, halo_in, cy_all, cz_all = new_sems(4)
+    mc_in, halo_in, cy_all = new_sems(3)
+    cz_from, cz_sems = new_sems(side - 1), new_sems(side - 1)
     send(mc_send, mc_recv, group(mc_send), mc_in, mate, x)
+
+    def hand_over_value(ks):
+        for k in ks:
+            block = gv.at[c, turn(a_me, side - k)]
+            arrive(block, v2_from[k - 1])
+            send(block, block, vc_sem, vc_all, mate, x)
+
+    near_first = far_first(side)[::-1]
+    hand_over_value(near_first[: side // 2])
 
     arrive(mc_recv, mc_in)
     core_entry = []
@@ -483,41 +498,7 @@
     for k in far_first(side):
         send(here, here, sem, cy_all, at(z, turn(y, k), c), x)
 
-    arrive(pz.at[pl.ds(0, (cols - 1) * planes)], p2_all)
-    p3_from = new_sems(side)
-    p3_sem, pc_sem = group(py.at[c, pl.ds(0, side - 1)]), group(py.at[c])
-    heading = 1 - 2 * c
-    ahead_steps, back_steps = side // 2, (side - 1) // 2
-
-    def along(k):
-        return lax.rem(y + k * heading + side, side)
-
-    def ring(step):
-        if step > 1:
-            for k, order, steps_there in (
-                (-(step - 1), step - 1, ahead_steps),
-                (step - 1, ahead_steps + step - 1, back_steps),
-            ):
-                if step - 1 <= steps_there:
-                    block = py.at[c, along(k)]
-                    arrive(block, p3_from[order])
-                    send(block, block, pc_sem, pc_all, mate, x)
-        for k, order, steps_there, to in (
-            (-(step - 1), step, ahead_steps, 1),
-            (step - 1, ahead_steps + step, back_steps, -1),
-        ):
-            if step <= steps_there:
-                block = py.at[c, along(k)]
-                send(block, block, p3_sem, p3_from[order], at(z, along(to), c), x)
-
-    ring(1)
-    line = py.at[c, y]
-    send(line, line, pc_sem, pc_all, mate, x)
-
-    for k in reversed(far_first(side)):
-        block = gv.at[c, turn(a_me, side - k)]
-        arrive(block, v2_from[k - 1])
-        send(block, block, vc_sem, vc_all, mate, x)
+    hand_over_value(near_first[side // 2 :])
 
     arrive(gv.at[1 - c], vc_all)
 
@@ -551,11 +532,18 @@
         mz_all[pl.ds(slot_z + 4 + q, 1), :] = all_im
         mz_all[pl.ds(slot_z + 8 + q, 1), :] = all_span
     here = mz_all.at[pl.ds(slot_z, 12), :]
-    sem = group(mz_all.at[pl.ds(0, part_rows), :])
+    for k in range(side - 1, 0, -1):
+
+        @pl.when(z + k < side)
+        def _():
+            send(here, here, cz_sems[k - 1], cz_from[k - 1], at(lax.rem(z + k, side), y, c), x)
+
+    arrive(gp.at[c, a_me, pl.ds(0, side - 1)], p1_all)
+    line = gp.at[c, a_me]
+    sem, pc_sem = group(gp.at[c, pl.ds(0, side - 1)]), group(gp.at[c])
     for k in far_first(side):
-        send(here, here, sem, cz_all, at(turn(z, k), y, c), x)
-
-    ring(2)
+        send(line, line, sem, p2_from[k - 1], a_peer(turn(a_me, k)), x)
+    send(line, line, pc_sem, pc_all, mate, x)
 
     arrive(halo, halo_in)
 
@@ -577,6 +565,54 @@
     own_mean = nn(mix, jnp.full((LANES, LANES), 1.0 / LANES, F32), HIGHEST)
     lane_x = pl.multiple_of(x * LANES, LANES)
     mix_all[:, pl.ds(lane_x, LANES)] = (mix - own_mean).astype(BF16)
+    half = rows // 2
+    right, left = lax.rem(x + 1, cols), lax.rem(x + cols - 1, cols)
+    across = lax.rem(x + 2, cols)
+
+    class Spread:
+        def __init__(self, buffer):
+            self.buffer = buffer
+            self.sem = group(buffer.at[:, pl.ds(0, (cols - 1) * LANES)])
+            self.arrivals = new_sems(6 if cols > 2 else 2)
+
+        def part(self, col, first):
+            lanes = pl.ds(pl.multiple_of(col * LANES, LANES), LANES)
+            return self.buffer.at[pl.ds(0 if first else half, half), lanes]
+
+        def push(self, col, first, order, to):
+            block = self.part(col, first)
+            send(block, block, self.sem, self.arrivals[order], sp, to)
+
+        def pull(self, col, first, order):
+            arrive(self.part(col, first), self.arrivals[order])
+
+        def begin(self):
+            self.push(x, 1, 0, right)
+            if cols > 2:
+                self.push(x, 0, 2, left)
+            self.push(x, 0, 1, right)
+            if cols > 2:
+                self.push(x, 1, 3, left)
+
+        def pass_on(self):
+            if cols > 2:
+                self.pull(left, 1, 0)
+                self.push(left, 1, 4, right)
+                self.pull(right, 0, 2)
+                self.push(right, 0, 5, left)
+
+        def finish(self):
+            if cols == 2:
+                self.pull(left, 1, 0)
+            self.pull(left, 0, 1)
+            if cols > 2:
+                self.pull(right, 1, 3)
+                self.pull(across, 1, 4)
+                self.pull(across, 0, 5)
+
+    mix_spread = Spread(mix_all)
+    mix_spread.begin()
+
     ones = jnp.ones((8, LANES), F32)
     row_st = ids((8, rows), 0)
     sums = nt(ones, mix, HIGHEST)
@@ -588,57 +624,14 @@
     sem = group(st_all.at[pl.ds(0, cols - 1)])
     for k in far_first(cols):
         send(here, here, sem, st_in, sp, lax.rem(x + k, cols))
-    half = rows // 2
-    right, left = lax.rem(x + 1, cols), lax.rem(x + cols - 1, cols)
-    across = lax.rem(x + 2, cols)
-
-    class Spread:
-        def __init__(self, buffer):
-            self.buffer = buffer
-            self.sem = group(buffer.at[:, pl.ds(0, (cols - 1) * LANES)])
-            self.arrivals = new_sems(6 if cols > 2 else 2)
-
-        def part(self, col, first):
-            lanes = pl.ds(pl.multiple_of(col * LANES, LANES), LANES)
-            return self.buffer.at[pl.ds(0 if first else half, half), lanes]
-
-        def push(self, col, first, order, to):
-            block = self.part(col, first)
-            send(block, block, self.sem, self.arrivals[order], sp, to)
-
-        def pull(self, col, first, order):
-            arrive(self.part(col, first), self.arrivals[order])
-
-        def begin(self):
-            self.push(x, 1, 0, right)
-            if cols > 2:
-                self.push(x, 0, 2, left)
-            self.push(x, 0, 1, right)
-            if cols > 2:
-                self.push(x, 1, 3, left)
-
-        def pass_on(self):
-            if cols > 2:
-                self.pull(left, 1, 0)
-                self.push(left, 1, 4, right)
-                self.pull(right, 0, 2)
-                self.push(right, 0, 5, left)
-
-        def finish(self):
-            if cols == 2:
-                self.pull(left, 1, 0)
-            self.pull(left, 0, 1)
-            if cols > 2:
-                self.pull(right, 1, 3)
-                self.pull(across, 1, 4)
-                self.pull(across, 0, 5)
-
-    mix_spread = Spread(mix_all)
-    mix_spread.begin()
-
-    ring(3)
-
-    arrive(mz_all.at[pl.ds(0, part_rows), :], cz_all)
+
+    for k in range(1, side):
+
+        @pl.when(z >= k)
+        def _():
+            from_slot = pl.multiple_of(lax.rem(z + side - k, side) * 16, 16)
+            arrive(mz_all.at[pl.ds(from_slot, 12), :], cz_from[k - 1])
+
 
     begin = []
     for q in range(4):
@@ -655,8 +648,6 @@
         begin.append(h_re * s_re - h_im * s_im + starts[q][0])
         begin.append(h_re * s_im + h_im * s_re + starts[q][1])
 
-    ring(4)
-
     def state_rows(j, carry):
         r = pl.ds(pl.multiple_of(j * 8, 8), 8)
         new = []
@@ -673,6 +664,8 @@
 
     lax.fori_loop(0, steps, state_rows, tuple(begin), unroll=2)
 
+    mix_spread.pass_on()
+
     def read_rows(r):
         first, rest = split_two(mm[r, :])
         total = nt(first, out_blocks[...])
@@ -689,12 +682,8 @@
     lax.fori_loop(0, steps, back_rows, 0, unroll=8)
     state_all[:, pl.ds(lane_x, LANES)] = drv[...].astype(BF16)
 
-    mix_spread.pass_on()
     state_spread = Spread(state_all)
     state_spread.begin()
-
-    for step in range(5, ahead_steps + 2):
-        ring(step)
 
     arrive(st_all.at[pl.ds(0, cols - 1)], st_in)
     channels = cols * LANES
@@ -718,23 +707,28 @@
 
     apply_norm(x)
 
+    for k in reversed(far_first(side)):
+        block = gp.at[c, turn(a_me, side - k)]
+        arrive(block, p2_from[k - 1])
+        send(block, block, pc_sem, pc_all, mate, x)
+
+    mix_spread.finish()
+
     state_spread.pass_on()
-
-    mix_spread.finish()
 
     for k in range(1, cols):
         apply_norm(lax.rem(x + k, cols))
 
-    arrive(py.at[1 - c], pc_all)
-
-    def place_out(b, carry):
-        for core in range(2):
-            for col in range(cols):
-                for plane in range(planes):
-                    r = pl.ds(pl.multiple_of((plane * side + b) * 32 + core * 16, 16), 16)
-                    piece = py[core, b, col, plane]
-                    wo_conv[r, pl.ds(col * LANES, LANES)] = piece[:, :LANES]
-                    wo_state[r, pl.ds(col * LANES, LANES)] = piece[:, LANES:]
+    arrive(gp.at[1 - c], pc_all)
+
+    def place_out(line_y, carry):
+        for plane_z in range(side):
+            plane, col = divmod((plane_z + side - shift) % side, cols)
+            for core in range(2):
+                r = pl.ds(pl.multiple_of((plane * side + line_y) * 32 + core * 16, 16), 16)
+                piece = gp[1, line_y, plane_z] if core else gp[0, plane_z, line_y]
+                wo_conv[r, pl.ds(col * LANES, LANES)] = piece[:, :LANES]
+                wo_state[r, pl.ds(col * LANES, LANES)] = piece[:, LANES:]
         return carry
 
     lax.fori_loop(0, side, place_out, 0)
@@ -753,12 +747,19 @@
 
     for total, sem in outgoing:
         copy(total, total, sem, sem, mate, x).wait_send()
+    for k in range(1, side):
+
+        @pl.when(z + k < side)
+        def _():
+            block = mz_all.at[pl.ds(slot_z, 12), :]
+            copy(block, block, cz_sems[k - 1], cz_sems[k - 1], mate, x).wait_send()
+
     assert next(free, None) is None
 
 
 def sem_count(side, cols):
-    operands, groups = 17, 17
-    return operands + groups + 2 * (side - 1) + side + 3 + 4 + 4 + 1 + 2 * (6 if cols > 2 else 2)
+    operands, groups = 17, 16
+    return operands + groups + 5 * (side - 1) + 3 + 4 + 3 + 1 + 2 * (6 if cols > 2 else 2)
 
 
 def on_device(
@@ -813,8 +814,8 @@
             pltpu.VMEM((rows, depth), BF16),
             pltpu.VMEM((2, side, side, 16, LANES), BF16),
             pltpu.VMEM((2, side, side, 16, 2 * LANES), BF16),
-            pltpu.VMEM((side, 16, 2 * LANES), BF16),
-            pltpu.VMEM((2, side, cols, planes, 16, 2 * LANES), BF16),
+            pltpu.VMEM((16, 2 * LANES), BF16),
+            pltpu.VMEM((2, side, side, 16, 2 * LANES), BF16),
             pltpu.VMEM((depth, LANES), BF16),
             pltpu.VMEM((depth, 2 * LANES), BF16),
             pltpu.VMEM((out_cols, cols * LANES), BF16),

time: 54.9 us -> 52.1 us (0.949)
  the two profiles are of different devices: /device:TPU:2 before, /device:TPU:8 now
where the time goes in v3:
time: 52.1 us; the launch traced here: 52 us
  Pallas kernels  51.2 us (98%)
  local copies, waits for them, and re-layouts  0.8 us (2%)
    pallas_call x1, Pallas kernels, on_device(): pl.pallas_call(functools.partial(kernel, (side, cols)), out_shape=pltpu.V...  51.2 us

profile of v3, /device:TPU:8, one launch (start us, length us, event | category | flops | bytes accessed | tf_op | source)
XLA Modules:
  0.0 52.0 jit_solution(15362380109021915880)
XLA Ops:
  0.0 51.2 %shard_map.163 = bf16[512,512]{1,0:T(8,128)(2,1)S(1)} custom-call(bf16[512,2048]{1,0:T(8,128)(2,1)} %tokens_hbm.1, bf16[16,128]{1,0:T(8,128)(2,1)} %value_hbm.1, bf16[16,128]{1,0:T(8,128)(2,1)} %gate_hbm.1, bf16[16,128]{1,0:T(8,128)(2,1)} %drive_hbm.1, bf16[16,128]{1,0:T(8,128)(2,1)} %bitcast.16, bf16[16,128]{1,0:T(8,128)(2,1)} %bitcast.17, ...), custom_call_target="tpu_custom_call" | custom-call | tf_op jit(solution)/shard_map/pallas_call | solution.py:806
  51.2 0.8 %copy.19 = bf16[512,512]{1,0:T(8,128)(2,1)} copy(bf16[512,512]{1,0:T(8,128)(2,1)S(1)} %shard_map.163) | data formatting | bytes 1048576
